TPU v7x, 128 devices: a whole 4x4x4 slice. The times are simulated.
128 devices in a mesh: sp: 16 (over z, x), tp: 8 (over y, core).
Axes of the slice: x: 4, y: 4, z: 4, core: 2. Of those that a mesh axis runs over, the one named last changes fastest.
Arguments:
- queries: bfloat16 [16384, 1024], P('sp', 'tp'), may hold values from -75 to 75
- key_rows: bfloat16 [16384, 1024], P('sp', 'tp'), may hold values from -4 to 4
- value_rows: bfloat16 [16384, 1024], P('sp', 'tp'), may hold values from -6 to 6
- cum_gate: float32 [16, 16384], P('tp'), may hold values from -2342 to 0, as said below
- residual: bfloat16 [16384, 2048], P(('sp', 'tp')), may hold values from -6 to 6
- out_weight: bfloat16 [1024, 2048], replicated, may hold values from -0.1875 to 0.1875
- gain_mix: float32 [2048], replicated, may hold values from 0.1 to 1.9
- gain_pre: float32 [2048], replicated, may hold values from 0.1 to 1.9
- gain_post: float32 [2048], replicated, may hold values from 0.1 to 1.9
- route_ids: int32 [16384, 2], P(('sp', 'tp')), may hold values from 0 to 127, all different within a row; in each aligned block of 128 rows (0 to 127, 128 to 255, ...) at most 3 rows name the same one
- route_weight: float32 [16384, 2], P(('sp', 'tp')), may hold values from 0.2 to 1
- w_gate: bfloat16 [128, 2048, 512], P(('sp', 'tp')), may hold values from -0.125 to 0.125
- w_up: bfloat16 [128, 2048, 512], P(('sp', 'tp')), may hold values from -0.125 to 0.125
- w_down: bfloat16 [128, 512, 2048], P(('sp', 'tp')), may hold values from -0.25 to 0.25
Outputs:
- layer_out: bfloat16 [16384, 2048], P(('sp', 'tp'))
Inputs may be any that keep to these rules, and one draw needn't show every extreme that they name: `route_ids`: each row names 2 different experts; in the rows of one device no expert is named more than 3 times, a bound that some block reaches. `cum_gate`: along the positions each head's values never rise.
All inputs are finite; a program needn't handle non-finite values.
Results may differ from a plain program's by a relative error of at most 0.018.
Values may be sent and summed in bfloat16 or wider, within the bound.
A program may use at most 64 MiB of HBM per device.

v0:
```python
import math

import jax
import jax.numpy as jnp
from jax import lax
from jax.sharding import PartitionSpec as P

HEAD_DIM = 64


NORM_EPS = 1e-06
MASKED = -1e30


def rms_scale(rows, gain):
    mean_sq = jnp.mean(rows * rows, axis=-1, keepdims=True)
    return rows * lax.rsqrt(mean_sq + NORM_EPS) * gain


def attend(running, queries, gate_q, q_start, key_part, value_part, gate_k, k_start):
    row_peak, row_total, weighted = running
    scores = jnp.einsum(
        "qhd,khd->hqk", queries, key_part, preferred_element_type=jnp.float32
    ) * HEAD_DIM ** (-0.5)
    scores = scores + gate_q[:, :, None] - gate_k[:, None, :]
    query_pos = q_start + lax.iota(jnp.int32, queries.shape[0])
    key_pos = k_start + lax.iota(jnp.int32, key_part.shape[0])
    allowed = (key_pos[None, :] <= query_pos[:, None])[None]
    scores = jnp.where(allowed, scores, MASKED)
    new_peak = jnp.maximum(row_peak, jnp.max(scores, axis=-1))
    unnorm = jnp.where(allowed, jnp.exp(scores - new_peak[..., None]), 0.0)
    rescale = jnp.exp(row_peak - new_peak)
    row_total = row_total * rescale + jnp.sum(unnorm, axis=-1)
    weighted = weighted * rescale.T[:, :, None] + jnp.einsum(
        "hqk,khd->qhd", unnorm.astype(jnp.bfloat16), value_part, preferred_element_type=jnp.float32
    )
    return (new_peak, row_total, weighted)


def local(
    queries,
    key_rows,
    value_rows,
    cum_gate,
    residual,
    out_weight,
    gain_mix,
    gain_pre,
    gain_post,
    route_ids,
    route_weight,
    w_gate,
    w_up,
    w_down,
):
    tok_dev, feature_width = queries.shape
    local_heads = feature_width // HEAD_DIM
    my_start = lax.axis_index("sp") * tok_dev
    query_heads = queries.reshape(tok_dev, local_heads, HEAD_DIM)
    gate_q = lax.dynamic_slice_in_dim(cum_gate, my_start, tok_dev, 1)
    initial = (
        jnp.full((local_heads, tok_dev), MASKED, jnp.float32),
        jnp.zeros((local_heads, tok_dev), jnp.float32),
        jnp.zeros((tok_dev, local_heads, HEAD_DIM), jnp.float32),
    )
    paired = jnp.stack((key_rows, value_rows))

    def consume(running, key_part, value_part, k_start):
        row_count = key_part.shape[0]
        gate_k = lax.dynamic_slice_in_dim(cum_gate, k_start, row_count, 1)
        return attend(
            running,
            query_heads,
            gate_q,
            my_start,
            key_part.reshape(row_count, local_heads, HEAD_DIM),
            value_part.reshape(row_count, local_heads, HEAD_DIM),
            gate_k,
            k_start,
        )

    running = initial
    piece = lax.all_gather(paired, "sp", axis=1, tiled=True)
    row_count = piece.shape[1]
    span_rows = math.gcd(row_count, tok_dev)

    def single(block_index, running):
        offset = block_index * span_rows
        part = lax.dynamic_slice_in_dim(piece, offset, span_rows, 1)
        return lax.cond(
            offset < my_start + tok_dev,
            lambda state_now: consume(state_now, part[0], part[1], offset),
            lambda state_now: state_now,
            running,
        )

    running = lax.fori_loop(0, row_count // span_rows, single, running)
    row_peak, row_total, weighted = running
    attended = (
        (weighted / row_total.T[:, :, None]).astype(jnp.bfloat16).reshape(tok_dev, feature_width)
    )
    head_rows = lax.all_to_all(attended, "tp", split_axis=0, concat_axis=1, tiled=True)
    projected = jnp.dot(head_rows, out_weight, preferred_element_type=jnp.float32)
    stream = (residual.astype(jnp.float32) + rms_scale(projected, gain_mix)).astype(jnp.bfloat16)
    stream_wide = lax.optimization_barrier(stream).astype(jnp.float32)
    normed = rms_scale(stream_wide, gain_pre).astype(jnp.bfloat16)
    rows_dev, top_count = route_ids.shape
    model_width = normed.shape[1]
    experts_all = lax.axis_size("sp") * lax.axis_size("tp")
    capacity = max(2, (4 * rows_dev * top_count + 3 * experts_all - 1) // (3 * experts_all))
    flat_ids = route_ids.reshape(-1)
    onehot = (flat_ids[:, None] == lax.iota(jnp.int32, experts_all)[None, :]).astype(jnp.int32)
    slot_rank = jnp.sum(jnp.cumsum(onehot, axis=0) * onehot, axis=1) - 1
    slot_index = flat_ids * capacity + slot_rank
    spread = jnp.repeat(normed, top_count, axis=0)
    outgoing = (
        jnp.zeros((experts_all * capacity, model_width), jnp.bfloat16).at[slot_index].set(spread)
    )
    outgoing = outgoing.reshape(experts_all, capacity, model_width)
    arrived = lax.all_to_all(outgoing, ("sp", "tp"), split_axis=0, concat_axis=0, tiled=True)
    sources, slots, width_here = arrived.shape
    flat_rows = arrived.reshape(sources * slots, width_here)
    gate_act = jnp.dot(flat_rows, w_gate[0], preferred_element_type=jnp.float32)
    up_act = jnp.dot(flat_rows, w_up[0], preferred_element_type=jnp.float32)
    hidden = (jax.nn.silu(gate_act) * up_act).astype(jnp.bfloat16)
    expert_out = jnp.dot(hidden, w_down[0], preferred_element_type=jnp.float32).astype(jnp.bfloat16)
    returned = lax.all_to_all(
        expert_out.reshape(sources, slots, width_here),
        ("sp", "tp"),
        split_axis=0,
        concat_axis=0,
        tiled=True,
    )
    picked = returned.reshape(experts_all * capacity, model_width)[slot_index]
    picked = picked.reshape(rows_dev, top_count, model_width).astype(jnp.float32)
    combined = jnp.sum(picked * route_weight[:, :, None], axis=1)
    return (stream_wide + rms_scale(combined, gain_post)).astype(jnp.bfloat16)


def solution(mesh):
    return jax.shard_map(
        local,
        mesh=mesh,
        in_specs=(
            P("sp", "tp"),
            P("sp", "tp"),
            P("sp", "tp"),
            P("tp", None),
            P(("sp", "tp"), None),
            P(),
            P(),
            P(),
            P(),
            P(("sp", "tp"), None),
            P(("sp", "tp"), None),
            P(("sp", "tp"), None, None),
            P(("sp", "tp"), None, None),
            P(("sp", "tp"), None, None),
        ),
        out_specs=P(("sp", "tp"), None),
        check_vma=False,
    )
```

profile of v0, /device:TPU:1, one launch (start us, length us, event | category | flops | bytes accessed | tf_op | source)
XLA Modules:
  0.0 409.1 jit_solution(8245087762462546506)
XLA Ops:
  6.5 0.0 copy-start
  6.5 0.0 copy-start.5
  6.5 0.0 all-gather.2.cloned.1.call-start
  6.5 1.2 copy.42
  7.8 1.1 copy.43
  8.9 0.8 pad_maximum_fusion
  9.7 0.0 all-gather.2.cloned.1.call-update
  9.8 0.8 copy.47
  10.5 0.1 eq.29
  10.7 0.1 eq.25
  10.8 1.1 copy.44
  11.9 0.1 copy.49
  12.0 0.2 fusion.41
  12.3 0.7 constant_dynamic-slice_fusion.3
  13.0 0.2 fusion.42
  13.2 0.0 copy-done.5
  13.2 70.6 %all-gather.2.cloned.1.call-done = bf16[2,16384,128]{1,2,0:T(8,128)(2,1)} async-done(((bf16[2,1024,128]{1,2,0:T(8,128)(2,1)}), bf16[2,16384,128]{1,2,0:T(8,128)(2,1)}) %all-gather.2.cloned.1.call-update) | async-done | bytes 8388624 | tf_op jit(solution)/shard_map/all_gather | solution.py:83
  84.0 11.8 %while.18 = (s32[]{:T(128)}, f32[2,1024]{1,0:T(2,128)S(1)}, f32[2,1024]{1,0:T(2,128)S(1)}, f32[1024,2,64]{0,2,1:T(8,128)S(1)}, s32[]{:T(128)}, /*index=5*/s32[]{...) while((s32[]{:T(128)}, f32[2,1024]{1,0:T(2,128)S(1)}, ...), condition=%wide.region_5.6_spmd, body=%wide.region_0.5_spmd.sunk | while | flops 578035712 | bytes 32457040 | solution.py:97
  84.0 11.1 %conditional.2 = ((f32[2,1024]{1,0:T(2,128)S(1)}, f32[2,1024]{1,0:T(2,128)S(1)}, f32[1024,2,64]{0,2,1:T(8,128)S(1)})) conditional(s32[]{:T(128)} %convert_element_type.89, (f32[2,1024]{1,0:T(2,128)S(1)}, f32[2,1024]{1,0:T(2,128)S(1)}, f32[1024,2,64]{0,2,1:T(8,128)S(1)}) %tuple.52, (s32[]{:T(128)}, s32[]{:T(128)}, bf16[2,16384,128]{1,2,0:T(8,128)(2,1)}, ...), branch_computations={%region_1.0_spmd, %region_2.4_spmd} | conditional | flops 578035712 | bytes 32456802 | solution.py:90
  84.0 0.7 constant_dynamic-slice_fusion.1
  84.7 1.1 constant_dynamic-slice_fusion.2
  85.8 0.7 broadcast_compare_fusion
  86.4 2.4 fusion.2
  88.9 3.2 fusion.9
  92.1 3.0 fusion.1
  95.8 0.0 copy-start.1
  95.8 0.0 copy-start.2
  95.9 0.7 copy.45
  96.6 5.1 %all-to-all-start = ((bf16[8,128,128]{1,2,0:T(8,128)(2,1)}), bf16[8,128,128]{1,2,0:T(8,128)(2,1)S(1)}, u32[]{:S(2)}, u32[]{:S(2)}) async-start(bf16[8,128,128]{1,2,0:T(8,128)(2,1)} %copy.45), calls=%async_computation | async-start | bytes 524288 | tf_op jit(solution)/shard_map/all_to_all | solution.py:102
  101.8 0.0 copy-start.3
  101.8 0.1 copy.46
  101.9 0.1 mul.133
  102.0 6.2 %all-to-all-done = bf16[8,128,128]{1,2,0:T(8,128)(2,1)S(1)} async-done(((bf16[8,128,128]{1,2,0:T(8,128)(2,1)}), bf16[8,128,128]{1,2,0:T(8,128)(2,1)S(1)}, u32[]{:S(2)}, u32[]{:S(2)}) %all-to-all-start) | async-done | bytes 262176 | tf_op jit(solution)/shard_map/all_to_all | solution.py:102
  108.2 3.0 multiply_reduce_fusion.2
  111.3 0.0 copy-done.1
  111.3 0.0 copy-done.2
  111.3 0.2 add_convert_fusion
  111.5 0.2 fusion.27
  111.7 0.0 copy-done.3
  111.7 0.2 fusion.29
  111.9 1.7 broadcast_in_dim.62
  113.6 2.3 reshape.167
  115.8 4.1 %scatter_custom_fusion = bf16[384,2048]{1,0:T(8,128)(2,1)} fusion(s32[256]{0:T(256)S(1)} %bitcast.80, bf16[256,2048]{1,0:T(8,128)(2,1)} %reshape.167, bf16[]{:T(256)} %constant.98.clone.1), kind=kCustom, calls=%fused_computation.47 | custom fusion | bytes 1573376 | tf_op jit(solution)/shard_map/scatter | solution.py:117
  120.0 5.1 %reshape.150 = bf16[128,3,2048]{2,1,0:T(4,128)(2,1)} reshape(bf16[384,2048]{1,0:T(8,128)(2,1)} %scatter_custom_fusion) | data formatting | bytes 3145728 | tf_op jit(solution)/shard_map/reshape | solution.py:119
  125.1 202.5 %all_to_all.29 = bf16[128,3,2048]{2,1,0:T(4,128)(2,1)} all-to-all(bf16[128,3,2048]{2,1,0:T(4,128)(2,1)} %reshape.150), channel_id=1, replica_groups=mesh['sp'=16,'tp'=8] {'sp','tp'}, dimensions={0} | all-to-all | bytes 3145728 | tf_op jit(solution)/shard_map/all_to_all | solution.py:120
  327.6 5.0 %reshape.151 = bf16[384,2048]{1,0:T(8,128)(2,1)} reshape(bf16[128,3,2048]{2,1,0:T(4,128)(2,1)} %all_to_all.29) | data formatting | bytes 3145728 | tf_op jit(solution)/shard_map/reshape | solution.py:122
  332.7 3.9 fusion.19
  336.6 0.0 copy-done
  336.6 5.3 %convolution_convert_fusion = bf16[384,2048]{1,0:T(8,128)(2,1)} fusion(bf16[1,512,2048]{2,1,0:T(8,128)(2,1)S(1)} %copy-done, bf16[384,2048]{1,0:T(8,128)(2,1)} %reshape.151, bf16[1,2048,512]{2,1,0:T(8,128)(2,1)} %param.30, f32[384,512]{1,0:T(8,128)} %fusion.19), kind=kOutput, calls=%fused_computation.23 | convolution fusion | flops 1612578816 | bytes 8126464 | tf_op jit(solution)/shard_map/dot_general | solution.py:126
  341.9 0.0 copy-start.6
  341.9 5.2 %reshape.152 = bf16[128,3,2048]{2,1,0:T(4,128)(2,1)} reshape(bf16[384,2048]{1,0:T(8,128)(2,1)} %convolution_convert_fusion) | data formatting | bytes 3145728 | tf_op jit(solution)/shard_map/reshape | solution.py:128
  347.1 5.8 %all-to-all-start.2 = ((bf16[128,3,2048]{2,1,0:T(4,128)(2,1)}), bf16[128,3,2048]{2,1,0:T(4,128)(2,1)}, u32[]{:S(2)}, u32[]{:S(2)}) async-start(bf16[128,3,2048]{2,1,0:T(4,128)(2,1)} %reshape.152), calls=%async_computation.2 | async-start | bytes 4194304 | tf_op jit(solution)/shard_map/all_to_all | solution.py:127
  352.9 0.0 copy-done.6
  352.9 0.1 copy.51
  353.0 29.7 %all-to-all-done.2 = bf16[128,3,2048]{2,1,0:T(4,128)(2,1)} async-done(((bf16[128,3,2048]{2,1,0:T(4,128)(2,1)}), bf16[128,3,2048]{2,1,0:T(4,128)(2,1)}, u32[]{:S(2)}, u32[]{:S(2)}) %all-to-all-start.2) | async-done | bytes 1572896 | tf_op jit(solution)/shard_map/all_to_all | solution.py:127
  382.8 5.1 %reshape.153 = bf16[384,2048]{1,0:T(8,128)(2,1)} reshape(bf16[128,3,2048]{2,1,0:T(4,128)(2,1)} %all-to-all-done.2) | data formatting | bytes 3145728 | tf_op jit(solution)/shard_map/reshape | solution.py:134
  387.9 4.9 %gather_fusion = bf16[256,2048]{1,0:T(8,128)(2,1)} fusion(bf16[384,2048]{1,0:T(8,128)(2,1)} %reshape.153, s32[1024]{0:T(1024)S(1)} %pad_clamp_fusion), kind=kCustom, calls=%fused_computation | custom fusion | bytes 2098176 | tf_op jit(solution)/shard_map/gather | solution.py:134
  392.8 0.0 copy-start.4
  392.8 3.4 reshape.154
  396.2 4.8 %multiply_reduce_fusion = f32[128,2048]{1,0:T(8,128)S(1)} fusion(f32[128,2,2048]{2,1,0:T(2,128)} %reshape.154, f32[128,2]{1,0:T(8,128)S(1)} %copy.51), kind=kLoop, calls=%fused_computation.29 | loop fusion | flops 786432 | bytes 3146752 | tf_op jit(solution)/shard_map/reduce_sum | solution.py:136
  401.0 0.2 multiply_reduce_fusion.1
  401.2 0.0 copy-done.4
  401.2 1.0 fusion.30
  (37 shorter events, 0.5 us)
Async XLA Ops:
  6.5 330.1 %copy-start = (bf16[1,512,2048]{2,1,0:T(8,128)(2,1)S(1)}, bf16[1,512,2048]{2,1,0:T(8,128)(2,1)}, u32[]{:S(2)}) copy-start(bf16[1,512,2048]{2,1,0:T(8,128)(2,1)} %param.31) | copy-start | bytes 6291460
  6.5 6.7 %copy-start.5 = (s32[128,2]{0,1:T(2,128)S(1)}, s32[128,2]{0,1:T(2,128)}, u32[]{:S(2)}) copy-start(s32[128,2]{0,1:T(2,128)} %param.27) | copy-start | bytes 3076
  6.5 77.3 %all-gather.2.cloned.1.call-start = ((), (), s32[]{:S(2)}) async-start(), calls=%async_computation.3 | async-start | bytes 8912896 | tf_op jit(solution)/shard_map/all_gather | solution.py:83
  95.8 15.5 %copy-start.1 = (bf16[128,2048]{1,0:T(8,128)(2,1)S(1)}, bf16[128,2048]{1,0:T(8,128)(2,1)}, u32[]{:S(2)}) copy-start(bf16[128,2048]{1,0:T(8,128)(2,1)} %param.22) | copy-start | bytes 1572868
  95.8 15.5 %copy-start.2 = (f32[2048]{0:T(1024)S(1)}, f32[2048]{0:T(1024)}, u32[]{:S(2)}) copy-start(f32[2048]{0:T(1024)} %param.24) | copy-start | bytes 24580
  96.6 11.6 %all-to-all-start = ((bf16[8,128,128]{1,2,0:T(8,128)(2,1)}), bf16[8,128,128]{1,2,0:T(8,128)(2,1)S(1)}, u32[]{:S(2)}, u32[]{:S(2)}) async-start(bf16[8,128,128]{1,2,0:T(8,128)(2,1)} %copy.45), calls=%async_computation | async-start | bytes 524288 | tf_op jit(solution)/shard_map/all_to_all | solution.py:102
  101.8 10.0 %copy-start.3 = (f32[2048]{0:T(1024)S(1)}, f32[2048]{0:T(1024)}, u32[]{:S(2)}) copy-start(f32[2048]{0:T(1024)} %param.25) | copy-start | bytes 24580
  341.9 11.0 %copy-start.6 = (f32[128,2]{0,1:T(2,128)S(1)}, f32[128,2]{0,1:T(2,128)}, u32[]{:S(2)}) copy-start(f32[128,2]{0,1:T(2,128)} %param.28) | copy-start | bytes 3076
  347.1 35.7 %all-to-all-start.2 = ((bf16[128,3,2048]{2,1,0:T(4,128)(2,1)}), bf16[128,3,2048]{2,1,0:T(4,128)(2,1)}, u32[]{:S(2)}, u32[]{:S(2)}) async-start(bf16[128,3,2048]{2,1,0:T(4,128)(2,1)} %reshape.152), calls=%async_computation.2 | async-start | bytes 4194304 | tf_op jit(solution)/shard_map/all_to_all | solution.py:127
  392.8 8.4 %copy-start.4 = (f32[2048]{0:T(1024)S(1)}, f32[2048]{0:T(1024)}, u32[]{:S(2)}) copy-start(f32[2048]{0:T(1024)} %param.26) | copy-start | bytes 24580
Sparse Core Ops, SparseCore 0:
  9.9 73.9 all-gather.1
where the time goes:
time: 411 us; the launch traced here: 409 us
  blocking collectives  203 us (49%)
  waiting for transfers between devices  107 us (26%)
  local copies, waits for them, and re-layouts  45.1 us (11%)
  matrix products  17.9 us (4%)
  between operations  13.6 us (3%)
  other arithmetic  11.6 us (3%)
  starting transfers between devices  10.9 us (3%)
    all_to_all x1, blocking collectives, local(): lax.all_to_all(outgoing, ('sp', 'tp'), split_axis=0, concat_axis=0, tiled...  203 us
    all_gather x1, waiting for transfers between devices, local(): piece = lax.all_gather(paired, 'sp', axis=1, tiled=True)  70.6 us
    all_to_all x1, waiting for transfers between devices, local(): lax.all_to_all(expert_out.reshape(sources, slots, width_here), ('sp', 'tp...  29.7 us
  transfers between devices with their start and end apart: 3, of which 3 were waited for; matrix products, arithmetic and copies ran while one was open for 1% of the time, Pallas kernels for 0%

commit v1 on v0

v1 whole, which is shorter than its diff:
```python
import functools
import math

import jax
import jax.numpy as jnp
from jax import lax
from jax.experimental import pallas as pl
from jax.experimental.pallas import tpu as pltpu
from jax.sharding import PartitionSpec as P

HEAD_DIM = 64


NORM_EPS = 1e-06
MASKED = -1e30
LOG2E = math.log2(math.e)
MESH = pl.DeviceIdType.MESH
TILE = 256


def rms_scale(rows, gain):
    mean_sq = jnp.mean(rows * rows, axis=-1, keepdims=True)
    return rows * lax.rsqrt(mean_sq + NORM_EPS) * gain


def where(sp, tp):
    return dict(device_id=(sp, tp), device_id_type=MESH)


def attention_kernel(
    q_ref, kv_ref, gate_ref, out_ref,
    q_in, q_use, kv_buf, v_one, gate_buf, peak, acc, o_out, o_in,
    kv_send, kv_recv, fwd_send, fwd_recv, q_send, q_recv, gate_send, gate_recv, o_send, o_recv,
):
    tok = q_ref.shape[0]
    half = tok // 2
    sp, tp = lax.axis_index("sp"), lax.axis_index("tp")
    z, x = sp // 4, sp % 4
    y, core = tp // 2, tp % 2
    partner = 2 * y + (1 - core)
    bz, bx = z // 2, x // 2
    zl, xl = jnp.minimum(z, 3 - z), jnp.minimum(x, 3 - x)
    zh, xh = 3 - zl, 3 - xl
    top_block = 4 * zh + xh
    pair_of_me = jnp.abs(bz - bx)
    owner = core == bz
    low_block = 4 * zl + jnp.where(core == 0, xl, xh)
    blocks = (low_block, 15 - low_block)

    def copy(src, dst, send_sem, recv_sem, dev_sp, dev_tp):
        return pltpu.make_async_remote_copy(
            src_ref=src, dst_ref=dst, send_sem=send_sem, recv_sem=recv_sem, **where(dev_sp, dev_tp)
        )

    q_copies = []
    for side in range(2):
        dest_sp = 4 * jnp.where(core == 0, zl, zh) + (xl if side == 0 else xh)
        dest_tp = 2 * y + pair_of_me
        mine = (dest_sp == sp) & (dest_tp == tp)
        cp = copy(q_ref, q_in.at[bz], q_send.at[side], q_recv.at[bz], dest_sp, dest_tp)
        q_copies.append((mine, cp))

        @pl.when(jnp.logical_not(mine))
        def _():
            cp.start()

        @pl.when(mine)
        def _():
            q_in[bz] = q_ref[...]

    gate_cp = copy(gate_ref, gate_buf, gate_send, gate_recv, sp, partner)
    own_cp = copy(kv_ref.at[bx], kv_buf.at[0], fwd_send.at[0], fwd_recv.at[0], sp, partner)

    @pl.when(owner)
    def _():
        gate_cp.start()
        own_cp.start()
        gate_buf[...] = gate_ref[...]
        kv_buf[0] = kv_ref[bx]

    def kv_out(k, d):
        dz, dx = k // 4, k % 4
        dest_z, dest_x = (z - dz + 4) % 4, (x - dx + 4) % 4
        top = 4 * jnp.maximum(dest_z, 3 - dest_z) + jnp.maximum(dest_x, 3 - dest_x)
        used = (dest_z // 2 == core) & (sp <= top)
        rows = pl.ds(d * half, half)
        return used, copy(
            kv_ref.at[dest_x // 2, rows], kv_buf.at[k, rows], kv_send.at[k, d], kv_recv.at[k],
            4 * dest_z + dest_x, 2 * y + d,
        )

    def source(k):
        return 4 * ((z + k // 4) % 4) + (x + k % 4) % 4

    def send_kv(k, carry):
        for d in range(2):
            used, cp = kv_out(k, d)

            @pl.when(used)
            def _():
                cp.start()

        return carry

    lax.fori_loop(1, 16, send_kv, 0)

    def arrived(k):
        rows = pl.ds(core * half, half)
        return copy(kv_buf.at[k, rows], kv_buf.at[k, rows], kv_send.at[0, 0], kv_recv.at[k], sp, partner)

    def passed(k):
        rows = pl.ds(core * half, half)
        return copy(kv_buf.at[k, rows], kv_buf.at[k, rows], fwd_send.at[k], fwd_recv.at[k], sp, partner)

    def expected(k):
        rows = pl.ds((1 - core) * half, half)
        return copy(kv_buf.at[k, rows], kv_buf.at[k, rows], fwd_send.at[k], fwd_recv.at[k], sp, partner)

    @pl.when(jnp.logical_not(owner))
    def _():
        gate_cp.wait_recv()

    peak[...] = jnp.full_like(peak, MASKED)
    acc[...] = jnp.zeros_like(acc)
    lane = lax.broadcasted_iota(jnp.int32, (TILE, 128), 1)
    for slot in range(2):
        from_x = jnp.where(core == slot, xl, xh)
        from_sp = 4 * (zl if slot == 0 else zh) + from_x
        local = (from_sp == sp) & owner

        @pl.when(jnp.logical_not(local))
        def _():
            copy(q_ref, q_in.at[slot], q_send.at[0], q_recv.at[slot], sp, partner).wait_recv()

        for r in range(tok // TILE):
            rows = pl.ds(r * TILE, TILE)
            wide = q_in[slot, rows, :].astype(jnp.float32) * (HEAD_DIM ** -0.5)
            wide = jnp.where(bx == 0, wide, pltpu.roll(wide, 64, 1))
            q_use[slot, rows, :] = jnp.where(lane < HEAD_DIM, wide, 0.0).astype(jnp.bfloat16)

    @pl.when(jnp.logical_not(owner))
    def _():
        own_cp.wait_recv()

    def tile(k, j, slot, row, keys, masked):
        rows = pl.ds(row, TILE)
        block = blocks[slot]
        base = gate_buf[bx, block, :, 0:1]
        bias = (base - gate_buf[bx, j, :, 0:keys]) * LOG2E
        s = lax.dot_general(
            q_use[slot, rows, :], kv_buf[k, 0:keys, :], (((1,), (1,)), ((), ())),
            preferred_element_type=jnp.float32,
        )
        s = s * LOG2E + bias
        if masked:
            q_pos = row + lax.broadcasted_iota(jnp.int32, (TILE, keys), 0)
            k_pos = lax.broadcasted_iota(jnp.int32, (TILE, keys), 1)
            s = jnp.where(k_pos <= q_pos, s, MASKED)
        old = peak[slot, rows, :]
        new = jnp.maximum(old, jnp.max(s, axis=1, keepdims=True))
        peak[slot, rows, :] = new
        p = jnp.exp2(s - new[:, 0:1]).astype(jnp.bfloat16)
        acc[slot, rows, :] = acc[slot, rows, :] * jnp.exp2(old - new) + jnp.dot(
            p, v_one[0:keys, :], preferred_element_type=jnp.float32
        )

    def step(k, carry):
        j = source(k)
        follow = source(k + 1)
        used = j <= top_block

        @pl.when((k < 15) & (follow <= top_block))
        def _():
            arrived(k + 1).wait_recv()
            passed(k + 1).start()

        @pl.when((k > 0) & used)
        def _():
            expected(k).wait_recv()

        @pl.when(used)
        def _():
            v_one[...] = jnp.where(
                lax.broadcasted_iota(jnp.int32, (tok, 128), 1) < HEAD_DIM,
                jnp.bfloat16(1.0), kv_buf[k],
            )

        for slot in range(2):
            @pl.when(j < blocks[slot])
            def _():
                def rows_of(r, c):
                    tile(k, j, slot, pl.multiple_of(r * TILE, TILE), tok, False)
                    return c

                lax.fori_loop(0, tok // TILE, rows_of, 0)

            @pl.when(j == blocks[slot])
            def _():
                for r in range(tok // TILE):
                    tile(k, j, slot, r * TILE, (r + 1) * TILE, True)

        return carry

    lax.fori_loop(0, 16, step, 0)

    lane64 = lax.broadcasted_iota(jnp.int32, (64, 128), 1)
    head = 4 * y + 2 * bz + bx

    def o_copy(slot, t):
        return copy(o_out.at[slot, t], o_in.at[head], o_send.at[slot, t], o_recv.at[head], blocks[slot], t)

    for slot in range(2):
        for t in range(8):
            o = acc[slot, t * 128:(t + 1) * 128, :]
            o = o / pltpu.roll(o, 64, 1)
            o_out[slot, t] = jnp.where(lane64 < 64, pltpu.roll(o[0:64], 64, 1), o[64:128]).astype(jnp.bfloat16)
    for slot in range(2):
        for t in range(8):
            mine = (blocks[slot] == sp) & (tp == t)

            @pl.when(mine)
            def _():
                o_in[head] = o_out[slot, t]

            @pl.when(jnp.logical_not(mine))
            def _():
                o_copy(slot, t).start()

    for h in range(16):
        r = h % 4
        from_z = zl if r < 2 else zh
        from_x = xl if r % 2 == 0 else xh
        mine = (4 * from_z + from_x == sp) & (2 * (h // 4) + pair_of_me == tp)

        @pl.when(jnp.logical_not(mine))
        def _():
            copy(o_out.at[0, 0], o_in.at[h], o_send.at[0, 0], o_recv.at[h], sp, partner).wait_recv()

    for h in range(0, 16, 2):
        a = o_in[h].astype(jnp.float32)
        b = o_in[h + 1].astype(jnp.float32)
        cols = slice(h * 64, h * 64 + 128)
        out_ref[0:64, cols] = jnp.where(lane64 < 64, a, pltpu.roll(b, 64, 1)).astype(jnp.bfloat16)
        out_ref[64:128, cols] = jnp.where(lane64 < 64, pltpu.roll(a, 64, 1), b).astype(jnp.bfloat16)

    for mine, cp in q_copies:
        @pl.when(jnp.logical_not(mine))
        def _():
            cp.wait_send()

    @pl.when(owner)
    def _():
        gate_cp.wait_send()
        own_cp.wait_send()

    def drain(k, carry):
        for d in range(2):
            used, cp = kv_out(k, d)

            @pl.when(used)
            def _():
                cp.wait_send()

        @pl.when(source(k) <= top_block)
        def _():
            passed(k).wait_send()

        return carry

    lax.fori_loop(1, 16, drain, 0)
    for slot in range(2):
        for t in range(8):
            @pl.when(jnp.logical_not((blocks[slot] == sp) & (tp == t)))
            def _():
                o_copy(slot, t).wait_send()


def attention(queries, key_rows, value_rows, cum_gate):
    tok = queries.shape[0]
    kv = jnp.stack([
        jnp.concatenate([key_rows[:, :64], value_rows[:, :64]], axis=1),
        jnp.concatenate([key_rows[:, 64:], value_rows[:, 64:]], axis=1),
    ])
    gate = cum_gate.reshape(2, 16, 1, tok)
    dma = pltpu.SemaphoreType.DMA
    return pl.pallas_call(
        attention_kernel,
        out_shape=jax.ShapeDtypeStruct((128, 1024), jnp.bfloat16),
        in_specs=[pl.BlockSpec(memory_space=pltpu.VMEM)] * 3,
        out_specs=pl.BlockSpec(memory_space=pltpu.VMEM),
        scratch_shapes=[
            pltpu.VMEM((2, tok, 128), jnp.bfloat16),
            pltpu.VMEM((2, tok, 128), jnp.bfloat16),
            pltpu.VMEM((16, tok, 128), jnp.bfloat16),
            pltpu.VMEM((tok, 128), jnp.bfloat16),
            pltpu.VMEM((2, 16, 1, tok), jnp.float32),
            pltpu.VMEM((2, tok, 128), jnp.float32),
            pltpu.VMEM((2, tok, 128), jnp.float32),
            pltpu.VMEM((2, 8, 64, 128), jnp.bfloat16),
            pltpu.VMEM((16, 64, 128), jnp.bfloat16),
            dma((16, 2)), dma((16,)), dma((16,)), dma((16,)), dma((2,)), dma((2,)), dma, dma,
            dma((2, 8)), dma((16,)),
        ],
        compiler_params=pltpu.CompilerParams(has_side_effects=True, vmem_limit_bytes=40 * 1024 * 1024),
        name="attention",
    )(queries, kv, gate)


def local(
    queries,
    key_rows,
    value_rows,
    cum_gate,
    residual,
    out_weight,
    gain_mix,
    gain_pre,
    gain_post,
    route_ids,
    route_weight,
    w_gate,
    w_up,
    w_down,
):
    head_rows = attention(queries, key_rows, value_rows, cum_gate)
    projected = jnp.dot(head_rows, out_weight, preferred_element_type=jnp.float32)
    stream = (residual.astype(jnp.float32) + rms_scale(projected, gain_mix)).astype(jnp.bfloat16)
    stream_wide = lax.optimization_barrier(stream).astype(jnp.float32)
    normed = rms_scale(stream_wide, gain_pre).astype(jnp.bfloat16)
    rows_dev, top_count = route_ids.shape
    model_width = normed.shape[1]
    experts_all = lax.axis_size("sp") * lax.axis_size("tp")
    capacity = max(2, (4 * rows_dev * top_count + 3 * experts_all - 1) // (3 * experts_all))
    flat_ids = route_ids.reshape(-1)
    onehot = (flat_ids[:, None] == lax.iota(jnp.int32, experts_all)[None, :]).astype(jnp.int32)
    slot_rank = jnp.sum(jnp.cumsum(onehot, axis=0) * onehot, axis=1) - 1
    slot_index = flat_ids * capacity + slot_rank
    spread = jnp.repeat(normed, top_count, axis=0)
    outgoing = (
        jnp.zeros((experts_all * capacity, model_width), jnp.bfloat16).at[slot_index].set(spread)
    )
    outgoing = outgoing.reshape(experts_all, capacity, model_width)
    arrived = lax.all_to_all(outgoing, ("sp", "tp"), split_axis=0, concat_axis=0, tiled=True)
    sources, slots, width_here = arrived.shape
    flat_rows = arrived.reshape(sources * slots, width_here)
    gate_act = jnp.dot(flat_rows, w_gate[0], preferred_element_type=jnp.float32)
    up_act = jnp.dot(flat_rows, w_up[0], preferred_element_type=jnp.float32)
    hidden = (jax.nn.silu(gate_act) * up_act).astype(jnp.bfloat16)
    expert_out = jnp.dot(hidden, w_down[0], preferred_element_type=jnp.float32).astype(jnp.bfloat16)
    returned = lax.all_to_all(
        expert_out.reshape(sources, slots, width_here),
        ("sp", "tp"),
        split_axis=0,
        concat_axis=0,
        tiled=True,
    )
    picked = returned.reshape(experts_all * capacity, model_width)[slot_index]
    picked = picked.reshape(rows_dev, top_count, model_width).astype(jnp.float32)
    combined = jnp.sum(picked * route_weight[:, :, None], axis=1)
    return (stream_wide + rms_scale(combined, gain_post)).astype(jnp.bfloat16)


def solution(mesh):
    return jax.shard_map(
        local,
        mesh=mesh,
        in_specs=(
            P("sp", "tp"),
            P("sp", "tp"),
            P("sp", "tp"),
            P("tp", None),
            P(("sp", "tp"), None),
            P(),
            P(),
            P(),
            P(),
            P(("sp", "tp"), None),
            P(("sp", "tp"), None),
            P(("sp", "tp"), None, None),
            P(("sp", "tp"), None, None),
            P(("sp", "tp"), None, None),
        ),
        out_specs=P(("sp", "tp"), None),
        check_vma=False,
    )
```

time: 411 us -> 240 us (0.58)
  blocking collectives: 203 us -> 35.8 us
  Pallas kernels: 0 us -> 105 us
  waiting for transfers between devices: 107 us -> 29.7 us
  between operations: 13.6 us -> 0.2 us
  matrix products: 17.9 us -> 11.3 us
  starting transfers between devices: 10.9 us -> 5.94 us
    all_to_all x1, blocking collectives: 203 us -> 35.8 us  [local(): lax.all_to_all(outgoing, ('sp', 'tp'), split_axis=0, concat_axis=0, tiled...]
    pallas_call x0 -> x1, Pallas kernels: none -> 105 us  [attention(): pl.pallas_call(attention_kernel, out_shape=jax.ShapeDtypeStruct((128, 102...]
    all_gather x1 -> x0, waiting for transfers between devices: 70.6 us -> none  [local(): piece = lax.all_gather(paired, 'sp', axis=1, tiled=True)]
    all_to_all x1 -> x0, waiting for transfers between devices: 6.2 us -> none  [local(): lax.all_to_all(attended, 'tp', split_axis=0, concat_axis=1, tiled=True)]
    dot_general x2 -> x0, matrix products: 5.63 us -> none  [the longest x1 3.21 us: attend(): jnp.einsum('hqk,khd->qhd', unnorm.astype(jnp.bfloat16), value_part, prefe...]
    all_to_all x1 -> x0, starting transfers between devices: 5.12 us -> none  [local(): lax.all_to_all(attended, 'tp', split_axis=0, concat_axis=1, tiled=True)]
  transfers between devices with their start and end apart: 3 -> 1, of which waited for: 3 -> 1; matrix products, arithmetic and copies ran while one was open for 1% -> 0% of each run, Pallas kernels for 0% -> 0%
where the time goes in v1:
time: 240 us; the launch traced here: 239 us
  Pallas kernels  105 us (44%)
  local copies, waits for them, and re-layouts  42 us (18%)
  blocking collectives  35.8 us (15%)
  waiting for transfers between devices  29.7 us (12%)
  matrix products  11.3 us (5%)
  other arithmetic  9.07 us (4%)
  starting transfers between devices  5.94 us (2%)
    pallas_call x1, Pallas kernels, attention(): pl.pallas_call(attention_kernel, out_shape=jax.ShapeDtypeStruct((128, 102...  105 us
    all_to_all x1, blocking collectives, local(): lax.all_to_all(outgoing, ('sp', 'tp'), split_axis=0, concat_axis=0, tiled...  35.8 us
    all_to_all x1, waiting for transfers between devices, local(): lax.all_to_all(expert_out.reshape(sources, slots, width_here), ('sp', 'tp...  29.7 us
    all_to_all x1, starting transfers between devices, local(): lax.all_to_all(expert_out.reshape(sources, slots, width_here), ('sp', 'tp...  5.94 us
    dot_general x1, matrix products, local(): jnp.dot(hidden, w_down[0], preferred_element_type=jnp.float32)  5.18 us
    reshape x1, local copies, waits for them, and re-layouts, local(): expert_out.reshape(sources, slots, width_here)  5.17 us
    reshape x1, local copies, waits for them, and re-layouts, local(): outgoing = outgoing.reshape(experts_all, capacity, model_width)  5.15 us
    reshape x1, local copies, waits for them, and re-layouts, local(): picked = returned.reshape(experts_all * capacity, model_width)[slot_index]  5.07 us
  transfers between devices with their start and end apart: 1, of which 1 were waited for; matrix products, arithmetic and copies ran while one was open for 0% of the time, Pallas kernels for 0%

profile of v1, /device:TPU:1, one launch (start us, length us, event | category | flops | bytes accessed | tf_op | source)
XLA Modules:
  0.0 239.3 jit_solution(2210098472672795771)
XLA Ops:
  0.0 0.0 copy-start
  0.0 0.0 copy-start.3
  0.0 0.9 copy.17
  0.9 0.1 eq.29
  1.1 0.1 eq.25
  1.2 0.7 broadcast_multiply_fusion
  1.9 1.2 fusion.30
  3.1 0.0 copy-start.1
  3.1 1.9 fusion.31
  5.0 0.0 copy-done.3
  5.0 0.2 reshape.100.gate_ref
  5.2 1.2 maximum_bitcast_fusion
  6.5 0.1 pad_maximum_fusion.kv_ref
  6.5 0.0 copy-done.1
  6.5 105.2 %attention.1 = bf16[128,1024]{1,0:T(8,128)(2,1)S(1)} custom-call(bf16[1024,128]{1,0:T(8,128)(2,1)S(1)} %copy-done.1, bf16[2,1024,128]{2,1,0:T(8,128)(2,1)S(1)} %pad_maximum_fusion.kv_ref, f32[2,16,1,1024]{3,2,1,0:T(1,128)S(1)} %reshape.100.gate_ref), custom_call_target="tpu_custom_call" | custom-call | tf_op jit(solution)/shard_map/attention/pallas_call | solution.py:286
  111.8 0.0 copy-start.2
  111.8 0.0 copy-start.4
  111.8 3.0 %multiply_reduce_fusion.2 = (f32[128]{0:T(128)S(1)}, f32[128,2048]{1,0:T(8,128)S(1)}) fusion(bf16[128,1024]{1,0:T(8,128)(2,1)S(1)} %attention.1, bf16[1024,2048]{1,0:T(8,128)(2,1)} %param.19), kind=kOutput, calls=%fused_computation.20 | convolution fusion | flops 537395072 | bytes 5505536 | tf_op jit(solution)/shard_map/dot_general | solution.py:326
  114.9 0.0 copy-start.5
  114.9 0.0 copy-done.2
  114.9 0.0 copy-done.4
  114.9 0.2 add_convert_fusion
  115.1 0.2 fusion.11
  115.3 0.2 copy-done.5
  115.6 0.2 fusion.13
  115.8 1.7 broadcast_in_dim.5
  117.4 2.3 reshape.120
  119.7 0.1 copy.19
  119.8 0.2 fusion.25
  120.1 0.2 fusion.26
  120.3 0.1 copy.16
  120.4 0.1 mul.98
  120.6 4.1 %scatter_custom_fusion = bf16[384,2048]{1,0:T(8,128)(2,1)} fusion(s32[256]{0:T(256)S(1)} %bitcast.39, bf16[256,2048]{1,0:T(8,128)(2,1)} %reshape.120, bf16[]{:T(256)} %constant.22.clone.1), kind=kCustom, calls=%fused_computation.26 | custom fusion | bytes 1573376 | tf_op jit(solution)/shard_map/scatter | solution.py:340
  124.7 5.1 %reshape.103 = bf16[128,3,2048]{2,1,0:T(4,128)(2,1)} reshape(bf16[384,2048]{1,0:T(8,128)(2,1)} %scatter_custom_fusion) | data formatting | bytes 3145728 | tf_op jit(solution)/shard_map/reshape | solution.py:342
  129.8 35.8 %all_to_all.10 = bf16[128,3,2048]{2,1,0:T(4,128)(2,1)} all-to-all(bf16[128,3,2048]{2,1,0:T(4,128)(2,1)} %reshape.103), channel_id=1, replica_groups=mesh['sp'=16,'tp'=8] {'sp','tp'}, dimensions={0} | all-to-all | bytes 3145728 | tf_op jit(solution)/shard_map/all_to_all | solution.py:343
  165.6 5.0 %reshape.104 = bf16[384,2048]{1,0:T(8,128)(2,1)} reshape(bf16[128,3,2048]{2,1,0:T(4,128)(2,1)} %all_to_all.10) | data formatting | bytes 3145728 | tf_op jit(solution)/shard_map/reshape | solution.py:345
  170.6 3.0 %fusion.3 = f32[384,512]{1,0:T(8,128)S(1)} fusion(bf16[384,2048]{1,0:T(8,128)(2,1)} %reshape.104, bf16[1,2048,512]{2,1,0:T(8,128)(2,1)} %param.25), kind=kOutput, calls=%fused_computation.6 | convolution fusion | flops 805306368 | bytes 4456448 | tf_op jit(solution)/shard_map/dot_general | solution.py:346
  173.7 0.0 copy-done
  173.7 5.2 %convolution_convert_fusion = bf16[384,2048]{1,0:T(8,128)(2,1)} fusion(bf16[1,512,2048]{2,1,0:T(8,128)(2,1)S(1)} %copy-done, bf16[384,2048]{1,0:T(8,128)(2,1)} %reshape.104, bf16[1,2048,512]{2,1,0:T(8,128)(2,1)} %param.26, f32[384,512]{1,0:T(8,128)S(1)} %fusion.3), kind=kOutput, calls=%fused_computation.2 | convolution fusion | flops 1612578816 | bytes 8126464 | tf_op jit(solution)/shard_map/dot_general | solution.py:349
  178.9 5.2 %reshape.105 = bf16[128,3,2048]{2,1,0:T(4,128)(2,1)} reshape(bf16[384,2048]{1,0:T(8,128)(2,1)} %convolution_convert_fusion) | data formatting | bytes 3145728 | tf_op jit(solution)/shard_map/reshape | solution.py:351
  184.0 0.0 copy-start.7
  184.0 5.9 %all-to-all-start.1 = ((bf16[128,3,2048]{2,1,0:T(4,128)(2,1)}), bf16[128,3,2048]{2,1,0:T(4,128)(2,1)}, u32[]{:S(2)}, u32[]{:S(2)}) async-start(bf16[128,3,2048]{2,1,0:T(4,128)(2,1)} %reshape.105), calls=%async_computation.1 | async-start | bytes 4194304 | tf_op jit(solution)/shard_map/all_to_all | solution.py:350
  190.0 0.0 copy-done.7
  190.0 0.1 copy.21
  190.1 29.7 %all-to-all-done.1 = bf16[128,3,2048]{2,1,0:T(4,128)(2,1)} async-done(((bf16[128,3,2048]{2,1,0:T(4,128)(2,1)}), bf16[128,3,2048]{2,1,0:T(4,128)(2,1)}, u32[]{:S(2)}, u32[]{:S(2)}) %all-to-all-start.1) | async-done | bytes 1572896 | tf_op jit(solution)/shard_map/all_to_all | solution.py:350
  219.9 5.1 %reshape.106 = bf16[384,2048]{1,0:T(8,128)(2,1)} reshape(bf16[128,3,2048]{2,1,0:T(4,128)(2,1)} %all-to-all-done.1) | data formatting | bytes 3145728 | tf_op jit(solution)/shard_map/reshape | solution.py:357
  224.9 4.9 %gather_fusion = bf16[256,2048]{1,0:T(8,128)(2,1)} fusion(bf16[384,2048]{1,0:T(8,128)(2,1)} %reshape.106, s32[1024]{0:T(1024)S(1)} %pad_clamp_fusion), kind=kCustom, calls=%fused_computation | custom fusion | bytes 2098176 | tf_op jit(solution)/shard_map/gather | solution.py:357
  229.9 3.4 %reshape.107 = f32[128,2,2048]{2,1,0:T(2,128)} reshape(bf16[256,2048]{1,0:T(8,128)(2,1)} %gather_fusion) | data formatting | bytes 3145728 | tf_op jit(solution)/shard_map/convert_element_type | solution.py:358
  233.3 0.0 copy-start.6
  233.3 4.8 %multiply_reduce_fusion = f32[128,2048]{1,0:T(8,128)S(1)} fusion(f32[128,2,2048]{2,1,0:T(2,128)} %reshape.107, f32[128,2]{1,0:T(8,128)S(1)} %copy.21), kind=kLoop, calls=%fused_computation.8 | loop fusion | flops 786432 | bytes 3146752 | tf_op jit(solution)/shard_map/reduce_sum | solution.py:359
  238.1 0.2 multiply_reduce_fusion.1
  238.2 0.0 copy-done.6
  238.2 1.0 fusion.14
  (12 shorter events, 0.1 us)
Async XLA Ops:
  0.0 173.7 %copy-start = (bf16[1,512,2048]{2,1,0:T(8,128)(2,1)S(1)}, bf16[1,512,2048]{2,1,0:T(8,128)(2,1)}, u32[]{:S(2)}) copy-start(bf16[1,512,2048]{2,1,0:T(8,128)(2,1)} %param.27) | copy-start | bytes 6291460
  0.0 5.0 %copy-start.3 = (f32[2,16384]{1,0:T(2,128)S(1)}, f32[2,16384]{1,0:T(2,128)}, u32[]{:S(2)}) copy-start(f32[2,16384]{1,0:T(2,128)} %param.17) | copy-start | bytes 393220
  3.1 3.4 %copy-start.1 = (bf16[1024,128]{1,0:T(8,128)(2,1)S(1)}, bf16[1024,128]{1,0:T(8,128)(2,1)}, u32[]{:S(2)}) copy-start(bf16[1024,128]{1,0:T(8,128)(2,1)} %q_ref.1) | copy-start | bytes 786436
  111.8 3.1 %copy-start.2 = (bf16[128,2048]{1,0:T(8,128)(2,1)S(1)}, bf16[128,2048]{1,0:T(8,128)(2,1)}, u32[]{:S(2)}) copy-start(bf16[128,2048]{1,0:T(8,128)(2,1)} %param.18) | copy-start | bytes 1572868
  111.8 3.1 %copy-start.4 = (f32[2048]{0:T(1024)S(1)}, f32[2048]{0:T(1024)}, u32[]{:S(2)}) copy-start(f32[2048]{0:T(1024)} %param.20) | copy-start | bytes 24580
  114.9 0.7 copy-start.5
  184.0 5.9 %copy-start.7 = (f32[128,2]{0,1:T(2,128)S(1)}, f32[128,2]{0,1:T(2,128)}, u32[]{:S(2)}) copy-start(f32[128,2]{0,1:T(2,128)} %param.24) | copy-start | bytes 3076
  184.0 35.8 %all-to-all-start.1 = ((bf16[128,3,2048]{2,1,0:T(4,128)(2,1)}), bf16[128,3,2048]{2,1,0:T(4,128)(2,1)}, u32[]{:S(2)}, u32[]{:S(2)}) async-start(bf16[128,3,2048]{2,1,0:T(4,128)(2,1)} %reshape.105), calls=%async_computation.1 | async-start | bytes 4194304 | tf_op jit(solution)/shard_map/all_to_all | solution.py:350
  233.3 5.0 %copy-start.6 = (f32[2048]{0:T(1024)S(1)}, f32[2048]{0:T(1024)}, u32[]{:S(2)}) copy-start(f32[2048]{0:T(1024)} %param.22) | copy-start | bytes 24580

commit v2 on v1

--- a/solution.py
+++ b/solution.py
@@ -16,6 +16,8 @@
 LOG2E = math.log2(math.e)
 MESH = pl.DeviceIdType.MESH
 TILE = 256
+SLOTS = 3
+GROUP = 32
 
 
 def rms_scale(rows, gain):
@@ -27,10 +29,25 @@
     return dict(device_id=(sp, tp), device_id_type=MESH)
 
 
-def attention_kernel(
-    q_ref, kv_ref, gate_ref, out_ref,
-    q_in, q_use, kv_buf, v_one, gate_buf, peak, acc, o_out, o_in,
+def offset_of(place):
+    low, mid, high = place % 4, (place // 4) % 4, (place // 16) % 4
+    return low, (mid + low) % 4, (high + mid + low) % 4, place // 64
+
+
+def place_of(dz, dx, dy, dcore):
+    mid = (dx - dz + 4) % 4
+    high = (dy - dz - mid + 8) % 4
+    return dz + 4 * mid + 16 * high + 64 * dcore
+
+
+def layer_kernel(
+    q_ref, kv_ref, gate_ref, residual_ref, mix_ref, pre_ref, post_ref,
+    token_ref, place_ref, weight_ref, ow_hbm, wg_hbm, wu_hbm, wd_hbm, out_ref,
+    q_in, q_use, kv_buf, v_one, gate_buf, peak, acc, o_out, o_in, att,
+    ow, wg, wu, wd, slab_wide, slab, stream, outgoing, arrived_rows, results, returned,
+    x_wide, x_rows, y_wide,
     kv_send, kv_recv, fwd_send, fwd_recv, q_send, q_recv, gate_send, gate_recv, o_send, o_recv,
+    w_sem, go_send, go_recv, back_send, back_recv,
 ):
     tok = q_ref.shape[0]
     half = tok // 2
@@ -52,6 +69,13 @@
             src_ref=src, dst_ref=dst, send_sem=send_sem, recv_sem=recv_sem, **where(dev_sp, dev_tp)
         )
 
+    loads = [
+        pltpu.make_async_copy(src, dst, w_sem.at[i])
+        for i, (src, dst) in enumerate(((ow_hbm, ow), (wg_hbm, wg), (wu_hbm, wu), (wd_hbm, wd)))
+    ]
+    for load in loads:
+        load.start()
+
     q_copies = []
     for side in range(2):
         dest_sp = 4 * jnp.where(core == 0, zl, zh) + (xl if side == 0 else xh)
@@ -240,8 +264,103 @@
         a = o_in[h].astype(jnp.float32)
         b = o_in[h + 1].astype(jnp.float32)
         cols = slice(h * 64, h * 64 + 128)
-        out_ref[0:64, cols] = jnp.where(lane64 < 64, a, pltpu.roll(b, 64, 1)).astype(jnp.bfloat16)
-        out_ref[64:128, cols] = jnp.where(lane64 < 64, pltpu.roll(a, 64, 1), b).astype(jnp.bfloat16)
+        att[0:64, cols] = jnp.where(lane64 < 64, a, pltpu.roll(b, 64, 1)).astype(jnp.bfloat16)
+        att[64:128, cols] = jnp.where(lane64 < 64, pltpu.roll(a, 64, 1), b).astype(jnp.bfloat16)
+
+    loads[0].wait()
+    projected = jnp.dot(att[...], ow[...], preferred_element_type=jnp.float32)
+    rows_in = residual_ref[...].astype(jnp.float32) + rms_scale(projected, mix_ref[...])
+    rows_in = rows_in.astype(jnp.bfloat16).astype(jnp.float32)
+    stream[...] = rows_in
+    normed = rms_scale(rows_in, pre_ref[...])
+    for c in range(16):
+        slab_wide[pl.ds(c, 128, stride=16), :] = normed[:, c * 128:(c + 1) * 128]
+    slab[...] = slab_wide[...].reshape(128, 16, 128).astype(jnp.bfloat16)
+
+    def fill(place, carry):
+        for s in range(SLOTS):
+            outgoing[place * SLOTS + s] = slab[token_ref[place * SLOTS + s]]
+        return carry
+
+    lax.fori_loop(0, 128, fill, 0, unroll=4)
+
+    def peer(place, sign):
+        dz, dx, dy, dcore = offset_of(place)
+        return (
+            4 * ((z + sign * dz + 4) % 4) + (x + sign * dx + 4) % 4,
+            2 * ((y + sign * dy + 4) % 4) + (core + dcore) % 2,
+        )
+
+    def go(place):
+        rows = pl.ds(place * SLOTS, SLOTS)
+        return copy(
+            outgoing.at[rows], arrived_rows.at[rows], go_send, go_recv.at[place // GROUP], *peer(place, 1)
+        )
+
+    def back(place):
+        rows = pl.ds(place * SLOTS, SLOTS)
+        return copy(
+            results.at[rows], returned.at[rows], back_send, back_recv.at[place // GROUP], *peer(place, -1)
+        )
+
+    def start_go(place, carry):
+        go(place).start()
+        return carry
+
+    lax.fori_loop(1, 128, start_go, 0)
+    arrived_rows[0:SLOTS] = outgoing[0:SLOTS]
+    for load in loads[1:]:
+        load.wait()
+
+    def group_rows(group):
+        first = SLOTS if group == 0 else group * GROUP * SLOTS
+        return pl.ds(first, (group + 1) * GROUP * SLOTS - first)
+
+    def expert_group(group):
+        rows = group_rows(group)
+        copy(
+            outgoing.at[rows], arrived_rows.at[rows], go_send, go_recv.at[group], sp, partner
+        ).wait_recv()
+        count = GROUP * SLOTS
+        first = group * count
+        x_wide[...] = arrived_rows[first:first + count].reshape(count * 16, 128).astype(jnp.float32)
+        for c in range(16):
+            x_rows[:, c * 128:(c + 1) * 128] = x_wide[pl.ds(c, count, stride=16), :].astype(jnp.bfloat16)
+        gate_act = jnp.dot(x_rows[...], wg[...], preferred_element_type=jnp.float32)
+        up_act = jnp.dot(x_rows[...], wu[...], preferred_element_type=jnp.float32)
+        hidden = (gate_act / (1.0 + jnp.exp(-gate_act)) * up_act).astype(jnp.bfloat16)
+        y = jnp.dot(hidden, wd[...], preferred_element_type=jnp.float32)
+        for c in range(16):
+            y_wide[pl.ds(c, count, stride=16), :] = y[:, c * 128:(c + 1) * 128]
+        results[first:first + count] = y_wide[...].reshape(count, 16, 128).astype(jnp.bfloat16)
+
+        def start_back(place, carry):
+            back(place).start()
+            return carry
+
+        lax.fori_loop(max(1, group * GROUP), (group + 1) * GROUP, start_back, 0)
+        if group == 0:
+            returned[0:SLOTS] = results[0:SLOTS]
+
+    for group in range(128 // GROUP):
+        expert_group(group)
+    for group in range(128 // GROUP):
+        rows = group_rows(group)
+        copy(
+            results.at[rows], returned.at[rows], back_send, back_recv.at[group], sp, partner
+        ).wait_recv()
+
+    def combine(n, carry):
+        first = returned[place_ref[n, 0]].astype(jnp.float32) * weight_ref[n, 0]
+        second = returned[place_ref[n, 1]].astype(jnp.float32) * weight_ref[n, 1]
+        slab_wide[pl.ds(pl.multiple_of(n * 16, 16), 16), :] = first + second
+        return carry
+
+    lax.fori_loop(0, 128, combine, 0, unroll=4)
+    combined = jnp.concatenate(
+        [slab_wide[pl.ds(c, 128, stride=16), :] for c in range(16)], axis=1
+    )
+    out_ref[...] = (stream[...] + rms_scale(combined, post_ref[...])).astype(jnp.bfloat16)
 
     for mine, cp in q_copies:
         @pl.when(jnp.logical_not(mine))
@@ -273,37 +392,9 @@
             @pl.when(jnp.logical_not((blocks[slot] == sp) & (tp == t)))
             def _():
                 o_copy(slot, t).wait_send()
-
-
-def attention(queries, key_rows, value_rows, cum_gate):
-    tok = queries.shape[0]
-    kv = jnp.stack([
-        jnp.concatenate([key_rows[:, :64], value_rows[:, :64]], axis=1),
-        jnp.concatenate([key_rows[:, 64:], value_rows[:, 64:]], axis=1),
-    ])
-    gate = cum_gate.reshape(2, 16, 1, tok)
-    dma = pltpu.SemaphoreType.DMA
-    return pl.pallas_call(
-        attention_kernel,
-        out_shape=jax.ShapeDtypeStruct((128, 1024), jnp.bfloat16),
-        in_specs=[pl.BlockSpec(memory_space=pltpu.VMEM)] * 3,
-        out_specs=pl.BlockSpec(memory_space=pltpu.VMEM),
-        scratch_shapes=[
-            pltpu.VMEM((2, tok, 128), jnp.bfloat16),
-            pltpu.VMEM((2, tok, 128), jnp.bfloat16),
-            pltpu.VMEM((16, tok, 128), jnp.bfloat16),
-            pltpu.VMEM((tok, 128), jnp.bfloat16),
-            pltpu.VMEM((2, 16, 1, tok), jnp.float32),
-            pltpu.VMEM((2, tok, 128), jnp.float32),
-            pltpu.VMEM((2, tok, 128), jnp.float32),
-            pltpu.VMEM((2, 8, 64, 128), jnp.bfloat16),
-            pltpu.VMEM((16, 64, 128), jnp.bfloat16),
-            dma((16, 2)), dma((16,)), dma((16,)), dma((16,)), dma((2,)), dma((2,)), dma, dma,
-            dma((2, 8)), dma((16,)),
-        ],
-        compiler_params=pltpu.CompilerParams(has_side_effects=True, vmem_limit_bytes=40 * 1024 * 1024),
-        name="attention",
-    )(queries, kv, gate)
+    everything = pl.ds(SLOTS, 127 * SLOTS)
+    copy(outgoing.at[everything], arrived_rows.at[everything], go_send, go_recv.at[0], sp, partner).wait_send()
+    copy(results.at[everything], returned.at[everything], back_send, back_recv.at[0], sp, partner).wait_send()
 
 
 def local(
@@ -322,42 +413,73 @@
     w_up,
     w_down,
 ):
-    head_rows = attention(queries, key_rows, value_rows, cum_gate)
-    projected = jnp.dot(head_rows, out_weight, preferred_element_type=jnp.float32)
-    stream = (residual.astype(jnp.float32) + rms_scale(projected, gain_mix)).astype(jnp.bfloat16)
-    stream_wide = lax.optimization_barrier(stream).astype(jnp.float32)
-    normed = rms_scale(stream_wide, gain_pre).astype(jnp.bfloat16)
-    rows_dev, top_count = route_ids.shape
-    model_width = normed.shape[1]
-    experts_all = lax.axis_size("sp") * lax.axis_size("tp")
-    capacity = max(2, (4 * rows_dev * top_count + 3 * experts_all - 1) // (3 * experts_all))
-    flat_ids = route_ids.reshape(-1)
-    onehot = (flat_ids[:, None] == lax.iota(jnp.int32, experts_all)[None, :]).astype(jnp.int32)
-    slot_rank = jnp.sum(jnp.cumsum(onehot, axis=0) * onehot, axis=1) - 1
-    slot_index = flat_ids * capacity + slot_rank
-    spread = jnp.repeat(normed, top_count, axis=0)
-    outgoing = (
-        jnp.zeros((experts_all * capacity, model_width), jnp.bfloat16).at[slot_index].set(spread)
+    tok = queries.shape[0]
+    kv = jnp.stack([
+        jnp.concatenate([key_rows[:, :64], value_rows[:, :64]], axis=1),
+        jnp.concatenate([key_rows[:, 64:], value_rows[:, 64:]], axis=1),
+    ])
+    gate = cum_gate.reshape(2, 16, 1, tok)
+    sp, tp = lax.axis_index("sp"), lax.axis_index("tp")
+    flat = route_ids.reshape(-1)
+    order = lax.iota(jnp.int32, flat.shape[0])
+    earlier = (flat[None, :] == flat[:, None]) & (order[None, :] < order[:, None])
+    rank = jnp.sum(earlier.astype(jnp.int32), axis=1)
+    e_sp, e_tp = flat // 8, flat % 8
+    place = place_of(
+        (e_sp // 4 - sp // 4 + 4) % 4,
+        (e_sp % 4 - sp % 4 + 4) % 4,
+        (e_tp // 2 - tp // 2 + 4) % 4,
+        (e_tp % 2 + tp % 2) % 2,
+    ) * SLOTS + rank
+    slots = lax.iota(jnp.int32, 128 * SLOTS)
+    token = jnp.sum(jnp.where(slots[:, None] == place[None, :], order[None, :] // 2, 0), axis=1)
+    dma = pltpu.SemaphoreType.DMA
+    vmem, smem, anywhere = (
+        pl.BlockSpec(memory_space=space) for space in (pltpu.VMEM, pltpu.SMEM, pl.ANY)
     )
-    outgoing = outgoing.reshape(experts_all, capacity, model_width)
-    arrived = lax.all_to_all(outgoing, ("sp", "tp"), split_axis=0, concat_axis=0, tiled=True)
-    sources, slots, width_here = arrived.shape
-    flat_rows = arrived.reshape(sources * slots, width_here)
-    gate_act = jnp.dot(flat_rows, w_gate[0], preferred_element_type=jnp.float32)
-    up_act = jnp.dot(flat_rows, w_up[0], preferred_element_type=jnp.float32)
-    hidden = (jax.nn.silu(gate_act) * up_act).astype(jnp.bfloat16)
-    expert_out = jnp.dot(hidden, w_down[0], preferred_element_type=jnp.float32).astype(jnp.bfloat16)
-    returned = lax.all_to_all(
-        expert_out.reshape(sources, slots, width_here),
-        ("sp", "tp"),
-        split_axis=0,
-        concat_axis=0,
-        tiled=True,
+    bf16, f32 = jnp.bfloat16, jnp.float32
+    rows = GROUP * SLOTS
+    return pl.pallas_call(
+        layer_kernel,
+        out_shape=jax.ShapeDtypeStruct((128, 2048), bf16),
+        in_specs=[vmem] * 7 + [smem] * 3 + [anywhere] * 4,
+        out_specs=vmem,
+        scratch_shapes=[
+            pltpu.VMEM((2, tok, 128), bf16),
+            pltpu.VMEM((2, tok, 128), bf16),
+            pltpu.VMEM((16, tok, 128), bf16),
+            pltpu.VMEM((tok, 128), bf16),
+            pltpu.VMEM((2, 16, 1, tok), f32),
+            pltpu.VMEM((2, tok, 128), f32),
+            pltpu.VMEM((2, tok, 128), f32),
+            pltpu.VMEM((2, 8, 64, 128), bf16),
+            pltpu.VMEM((16, 64, 128), bf16),
+            pltpu.VMEM((128, 1024), bf16),
+            pltpu.VMEM((1024, 2048), bf16),
+            pltpu.VMEM((2048, 512), bf16),
+            pltpu.VMEM((2048, 512), bf16),
+            pltpu.VMEM((512, 2048), bf16),
+            pltpu.VMEM((2048, 128), f32),
+            pltpu.VMEM((128, 16, 128), bf16),
+            pltpu.VMEM((128, 2048), f32),
+            pltpu.VMEM((128 * SLOTS, 16, 128), bf16),
+            pltpu.VMEM((128 * SLOTS, 16, 128), bf16),
+            pltpu.VMEM((128 * SLOTS, 16, 128), bf16),
+            pltpu.VMEM((128 * SLOTS, 16, 128), bf16),
+            pltpu.VMEM((rows * 16, 128), f32),
+            pltpu.VMEM((rows, 2048), bf16),
+            pltpu.VMEM((rows * 16, 128), f32),
+            dma((16, 2)), dma((16,)), dma((16,)), dma((16,)), dma((2,)), dma((2,)), dma, dma,
+            dma((2, 8)), dma((16,)),
+            dma((4,)), dma, dma((128 // GROUP,)), dma, dma((128 // GROUP,)),
+        ],
+        compiler_params=pltpu.CompilerParams(has_side_effects=True, vmem_limit_bytes=60 * 1024 * 1024),
+        name="layer",
+    )(
+        queries, kv, gate, residual, gain_mix.reshape(1, -1), gain_pre.reshape(1, -1),
+        gain_post.reshape(1, -1), token, place.reshape(128, 2), route_weight,
+        out_weight, w_gate[0], w_up[0], w_down[0],
     )
-    picked = returned.reshape(experts_all * capacity, model_width)[slot_index]
-    picked = picked.reshape(rows_dev, top_count, model_width).astype(jnp.float32)
-    combined = jnp.sum(picked * route_weight[:, :, None], axis=1)
-    return (stream_wide + rms_scale(combined, gain_post)).astype(jnp.bfloat16)
 
 
 def solution(mesh):

time: 240 us -> 161 us (0.67)
  Pallas kernels: 105 us -> 151 us
  blocking collectives: 35.8 us -> 0 us
  local copies, waits for them, and re-layouts: 42 us -> 6.42 us
  waiting for transfers between devices: 29.7 us -> 0 us
  matrix products: 11.3 us -> 0 us
  other arithmetic: 9.07 us -> 3.09 us
  starting transfers between devices: 5.94 us -> 0 us
    pallas_call x1, Pallas kernels: 105 us -> 151 us  [local(): pl.pallas_call(layer_kernel, out_shape=jax.ShapeDtypeStruct((128, 2048),...]
    all_to_all x1 -> x0, blocking collectives: 35.8 us -> none  [local(): lax.all_to_all(outgoing, ('sp', 'tp'), split_axis=0, concat_axis=0, tiled...]
    all_to_all x1 -> x0, waiting for transfers between devices: 29.7 us -> none  [local(): lax.all_to_all(expert_out.reshape(sources, slots, width_here), ('sp', 'tp...]
    reshape x6 -> x2, local copies, waits for them, and re-layouts: 22.9 us -> 0.99 us  [the longest x1 0.85 us: local(): gate = cum_gate.reshape(2, 16, 1, tok)]
    dot_general x3 -> x0, matrix products: 11.3 us -> none  [the longest x1 5.18 us: local(): jnp.dot(hidden, w_down[0], preferred_element_type=jnp.float32)]
    all_to_all x1 -> x0, starting transfers between devices: 5.94 us -> none  [local(): lax.all_to_all(expert_out.reshape(sources, slots, width_here), ('sp', 'tp...]
    gather x1 -> x0, local copies, waits for them, and re-layouts: 4.93 us -> none  [local(): picked = returned.reshape(experts_all * capacity, model_width)[slot_index]]
    reduce_sum x4 -> x2, other arithmetic: 5.33 us -> 0.9 us  [the longest x1 0.72 us: local(): jnp.sum(jnp.where(slots[:, None] == place[None, :], order[None, :] // 2,...]
  transfers between devices with their start and end apart: 1 -> 0, of which waited for: 1 -> 0; matrix products, arithmetic and copies ran while one was open for 0% -> 0% of each run, Pallas kernels for 0% -> 0%
where the time goes in v2:
time: 161 us
  Pallas kernels  151 us (94%)
  local copies, waits for them, and re-layouts  6.42 us (4%)
  other arithmetic  3.09 us (2%)
    pallas_call x1, Pallas kernels, local(): pl.pallas_call(layer_kernel, out_shape=jax.ShapeDtypeStruct((128, 2048),...  151 us

profile of v2, /device:TPU:1, one launch (start us, length us, event | category | flops | bytes accessed | tf_op | source)
XLA Modules:
  0.0 160.9 jit_solution(15288632424917057406)
XLA Ops:
  0.0 1.2 fusion.44
  1.2 0.0 copy-start
  1.2 0.0 copy-start.1
  1.2 0.0 copy-start.2
  1.2 1.2 fusion.43
  2.5 0.3 maximum_bitcast_fusion
  2.8 0.8 pad_maximum_fusion.kv_ref
  3.6 0.0 copy-done
  3.6 0.9 reshape.244.gate_ref
  4.5 0.0 copy-done.1
  4.5 0.1 copy.32
  4.6 0.1 reshape.248
  4.7 0.2 convert_reduce_fusion
  4.9 0.1 and_select_fusion
  5.0 0.7 select_reduce_fusion.token_ref
  5.7 0.1 reduce_sum.22
  5.9 0.1 copy.38
  6.0 1.0 fusion.21.place_ref
  7.0 0.0 copy-done.2
  7.0 0.7 copy.40.weight_ref
  7.7 151.3 %layer.1 = bf16[128,2048]{1,0:T(8,128)(2,1)} custom-call(bf16[1024,128]{1,0:T(8,128)(2,1)} %q_ref.1, bf16[2,1024,128]{2,1,0:T(8,128)(2,1)} %pad_maximum_fusion.kv_ref, f32[2,16,1,1024]{3,2,1,0:T(1,128)} %reshape.244.gate_ref, bf16[128,2048]{1,0:T(8,128)(2,1)} %residual_ref.1, f32[1,2048]{1,0:T(1,128)} %bitcast.13, f32[1,2048]{1,0:T(1,128)} %bitcast.14, ...), custom_call_target="tpu_custom_call" | custom-call | tf_op jit(solution)/shard_map/layer/pallas_call | solution.py:442
  159.0 1.9 %copy.50 = bf16[128,2048]{1,0:T(8,128)(2,1)} copy(bf16[128,2048]{1,0:T(8,128)(2,1)} %layer.1) | data formatting | bytes 1048576
  (1 shorter events, 0.0 us)
Async XLA Ops:
  1.2 2.4 %copy-start = (f32[2,16384]{1,0:T(2,128)S(1)}, f32[2,16384]{1,0:T(2,128)}, u32[]{:S(2)}) copy-start(f32[2,16384]{1,0:T(2,128)} %param.17) | copy-start | bytes 393220
  1.2 3.3 %copy-start.1 = (s32[128,2]{0,1:T(2,128)S(1)}, s32[128,2]{0,1:T(2,128)}, u32[]{:S(2)}) copy-start(s32[128,2]{0,1:T(2,128)} %param.23) | copy-start | bytes 3076
  1.2 5.8 %copy-start.2 = (f32[128,2]{0,1:T(2,128)S(1)}, f32[128,2]{0,1:T(2,128)}, u32[]{:S(2)}) copy-start(f32[128,2]{0,1:T(2,128)} %param.24) | copy-start | bytes 3076

commit v3 on v2

--- a/solution.py
+++ b/solution.py
@@ -16,6 +16,7 @@
 LOG2E = math.log2(math.e)
 MESH = pl.DeviceIdType.MESH
 TILE = 256
+QROWS = 256
 SLOTS = 3
 GROUP = 32
 
@@ -23,6 +24,13 @@
 def rms_scale(rows, gain):
     mean_sq = jnp.mean(rows * rows, axis=-1, keepdims=True)
     return rows * lax.rsqrt(mean_sq + NORM_EPS) * gain
+
+
+def split3(values):
+    first = values.astype(jnp.bfloat16).astype(jnp.float32)
+    second = (values - first).astype(jnp.bfloat16).astype(jnp.float32)
+    third = (values - first - second).astype(jnp.bfloat16).astype(jnp.float32)
+    return first, second, third
 
 
 def where(sp, tp):
@@ -43,13 +51,13 @@
 def layer_kernel(
     q_ref, kv_ref, gate_ref, residual_ref, mix_ref, pre_ref, post_ref,
     token_ref, place_ref, weight_ref, ow_hbm, wg_hbm, wu_hbm, wd_hbm, out_ref,
-    q_in, q_use, kv_buf, v_one, gate_buf, peak, acc, o_out, o_in, att,
+    q_in, q_use, kv_buf, gate_cols, k_aug, s_buf, v_one, gate_buf, peak, acc, o_out, o_in, att,
     ow, wg, wu, wd, slab_wide, slab, stream, outgoing, arrived_rows, results, returned,
     x_wide, x_rows, y_wide,
     kv_send, kv_recv, fwd_send, fwd_recv, q_send, q_recv, gate_send, gate_recv, o_send, o_recv,
     w_sem, go_send, go_recv, back_send, back_recv,
 ):
-    tok = q_ref.shape[0]
+    tok = kv_ref.shape[1]
     half = tok // 2
     sp, tp = lax.axis_index("sp"), lax.axis_index("tp")
     z, x = sp // 4, sp % 4
@@ -81,7 +89,7 @@
         dest_sp = 4 * jnp.where(core == 0, zl, zh) + (xl if side == 0 else xh)
         dest_tp = 2 * y + pair_of_me
         mine = (dest_sp == sp) & (dest_tp == tp)
-        cp = copy(q_ref, q_in.at[bz], q_send.at[side], q_recv.at[bz], dest_sp, dest_tp)
+        cp = copy(q_ref.at[side], q_in.at[bz], q_send.at[side], q_recv.at[bz], dest_sp, dest_tp)
         q_copies.append((mine, cp))
 
         @pl.when(jnp.logical_not(mine))
@@ -90,7 +98,7 @@
 
         @pl.when(mine)
         def _():
-            q_in[bz] = q_ref[...]
+            q_in[bz] = q_ref[side]
 
     gate_cp = copy(gate_ref, gate_buf, gate_send, gate_recv, sp, partner)
     own_cp = copy(kv_ref.at[bx], kv_buf.at[0], fwd_send.at[0], fwd_recv.at[0], sp, partner)
@@ -102,8 +110,11 @@
         gate_buf[...] = gate_ref[...]
         kv_buf[0] = kv_ref[bx]
 
+    def step_offset(k):
+        return (-1369213168 >> (2 * k)) & 3, (-1182141244 >> (2 * k)) & 3
+
     def kv_out(k, d):
-        dz, dx = k // 4, k % 4
+        dz, dx = step_offset(k)
         dest_z, dest_x = (z - dz + 4) % 4, (x - dx + 4) % 4
         top = 4 * jnp.maximum(dest_z, 3 - dest_z) + jnp.maximum(dest_x, 3 - dest_x)
         used = (dest_z // 2 == core) & (sp <= top)
@@ -114,7 +125,8 @@
         )
 
     def source(k):
-        return 4 * ((z + k // 4) % 4) + (x + k % 4) % 4
+        dz, dx = step_offset(k)
+        return 4 * ((z + dz) % 4) + (x + dx) % 4
 
     def send_kv(k, carry):
         for d in range(2):
@@ -126,7 +138,7 @@
 
         return carry
 
-    lax.fori_loop(1, 16, send_kv, 0)
+    lax.fori_loop(1, 9, send_kv, 0)
 
     def arrived(k):
         rows = pl.ds(core * half, half)
@@ -146,7 +158,26 @@
 
     peak[...] = jnp.full_like(peak, MASKED)
     acc[...] = jnp.zeros_like(acc)
-    lane = lax.broadcasted_iota(jnp.int32, (TILE, 128), 1)
+    lane = lax.broadcasted_iota(jnp.int32, (QROWS, 128), 1)
+    at_row = lax.broadcasted_iota(jnp.int32, (8, 128), 0)
+    at_lane = lax.broadcasted_iota(jnp.int32, (8, 128), 1)
+    put = jnp.where(
+        (at_lane == at_row + HEAD_DIM) & (at_row < 3) | (at_row == 3) & (at_lane >= HEAD_DIM + 3) & (at_lane < HEAD_DIM + 6),
+        1.0, 0.0,
+    ).astype(jnp.bfloat16)
+    row8 = lax.broadcasted_iota(jnp.int32, (8, tok), 0)
+
+    def columns(j, carry):
+        parts = split3(gate_buf[bx, j] * -LOG2E)
+        stack = jnp.where(row8 == 3, 1.0, 0.0)
+        for i in range(3):
+            stack = jnp.where(row8 == i, parts[i], stack)
+        gate_cols[j] = lax.dot_general(
+            stack.astype(jnp.bfloat16), put, (((0,), (0,)), ((), ())), preferred_element_type=jnp.float32
+        ).astype(jnp.bfloat16)
+        return carry
+
+    lax.fori_loop(0, 16, columns, 0)
     for slot in range(2):
         from_x = jnp.where(core == slot, xl, xh)
         from_sp = 4 * (zl if slot == 0 else zh) + from_x
@@ -154,43 +185,61 @@
 
         @pl.when(jnp.logical_not(local))
         def _():
-            copy(q_ref, q_in.at[slot], q_send.at[0], q_recv.at[slot], sp, partner).wait_recv()
-
-        for r in range(tok // TILE):
-            rows = pl.ds(r * TILE, TILE)
-            wide = q_in[slot, rows, :].astype(jnp.float32) * (HEAD_DIM ** -0.5)
-            wide = jnp.where(bx == 0, wide, pltpu.roll(wide, 64, 1))
-            q_use[slot, rows, :] = jnp.where(lane < HEAD_DIM, wide, 0.0).astype(jnp.bfloat16)
+            copy(q_ref.at[0], q_in.at[slot], q_send.at[0], q_recv.at[slot], sp, partner).wait_recv()
+
+        base = gate_buf[bx, blocks[slot], :, 0:1] * LOG2E
+        pieces = split3(base)
+        for r in range(tok // QROWS):
+            rows = pl.ds(r * QROWS, QROWS)
+            wide = q_in[slot, pl.ds(r * QROWS % half, QROWS), :].astype(jnp.float32) * (LOG2E * HEAD_DIM ** -0.5)
+            wide = wide if r * QROWS < half else pltpu.roll(wide, 64, 1)
+            high = jnp.where(lane < HEAD_DIM, wide, 0.0).astype(jnp.bfloat16)
+            low = (wide - high.astype(jnp.float32)).astype(jnp.bfloat16).astype(jnp.float32)
+            extra = jnp.where(lane < HEAD_DIM + 3, 1.0, 0.0)
+            for i in range(3):
+                extra = jnp.where(lane == HEAD_DIM + 3 + i, pieces[i], extra)
+            q_use[slot, rows, 0:128] = high
+            q_use[slot, rows, 128:256] = jnp.where(lane < HEAD_DIM, low, extra).astype(jnp.bfloat16)
 
     @pl.when(jnp.logical_not(owner))
     def _():
         own_cp.wait_recv()
 
-    def tile(k, j, slot, row, keys, masked):
-        rows = pl.ds(row, TILE)
-        block = blocks[slot]
-        base = gate_buf[bx, block, :, 0:1]
-        bias = (base - gate_buf[bx, j, :, 0:keys]) * LOG2E
-        s = lax.dot_general(
-            q_use[slot, rows, :], kv_buf[k, 0:keys, :], (((1,), (1,)), ((), ())),
-            preferred_element_type=jnp.float32,
-        )
-        s = s * LOG2E + bias
-        if masked:
-            q_pos = row + lax.broadcasted_iota(jnp.int32, (TILE, keys), 0)
-            k_pos = lax.broadcasted_iota(jnp.int32, (TILE, keys), 1)
-            s = jnp.where(k_pos <= q_pos, s, MASKED)
-        old = peak[slot, rows, :]
-        new = jnp.maximum(old, jnp.max(s, axis=1, keepdims=True))
-        peak[slot, rows, :] = new
-        p = jnp.exp2(s - new[:, 0:1]).astype(jnp.bfloat16)
-        acc[slot, rows, :] = acc[slot, rows, :] * jnp.exp2(old - new) + jnp.dot(
-            p, v_one[0:keys, :], preferred_element_type=jnp.float32
-        )
+    def attend(slot, diagonal):
+        tiles = tok // TILE
+        keys = [(r + 1) * TILE if diagonal else tok for r in range(tiles)]
+        olds, news = [], []
+        for i in range(tiles + 1):
+            if i < tiles:
+                rows = slice(i * TILE, (i + 1) * TILE)
+                s = lax.dot_general(
+                    q_use[slot, rows, :], k_aug[0:keys[i], :], (((1,), (1,)), ((), ())),
+                    preferred_element_type=jnp.float32,
+                )
+                if diagonal:
+                    q_pos = lax.broadcasted_iota(jnp.int32, (TILE, TILE), 0)
+                    k_pos = lax.broadcasted_iota(jnp.int32, (TILE, TILE), 1)
+                    last = jnp.where(k_pos <= q_pos, s[:, keys[i] - TILE:], MASKED)
+                    s = last if i == 0 else jnp.concatenate([s[:, :keys[i] - TILE], last], axis=1)
+                s_buf[i % s_buf.shape[0], :, 0:keys[i]] = s
+                olds.append(peak[slot, rows, :])
+                news.append(jnp.maximum(olds[i], jnp.max(s, axis=1, keepdims=True)))
+                peak[slot, rows, :] = news[i]
+            if i > 0:
+                r = i - 1
+                rows = slice(r * TILE, (r + 1) * TILE)
+                p = jnp.exp2(s_buf[r % s_buf.shape[0], :, 0:keys[r]] - news[r][:, 0:1]).astype(jnp.bfloat16)
+                acc[slot, rows, :] = acc[slot, rows, :] * jnp.exp2(olds[r] - news[r]) + jnp.dot(
+                    p, v_one[0:keys[r], :], preferred_element_type=jnp.float32
+                )
 
     def step(k, carry):
+        @pl.when(k < 7)
+        def _():
+            send_kv(k + 9, 0)
+
         j = source(k)
-        follow = source(k + 1)
+        follow = source(jnp.minimum(k + 1, 15))
         used = j <= top_block
 
         @pl.when((k < 15) & (follow <= top_block))
@@ -204,24 +253,20 @@
 
         @pl.when(used)
         def _():
-            v_one[...] = jnp.where(
-                lax.broadcasted_iota(jnp.int32, (tok, 128), 1) < HEAD_DIM,
-                jnp.bfloat16(1.0), kv_buf[k],
-            )
+            left = lax.broadcasted_iota(jnp.int32, (tok, 128), 1) < HEAD_DIM
+            rows_kv = kv_buf[k]
+            v_one[...] = jnp.where(left, jnp.bfloat16(1.0), rows_kv)
+            k_aug[:, 0:128] = rows_kv
+            k_aug[:, 128:256] = jnp.where(left, rows_kv, gate_cols[j])
 
         for slot in range(2):
             @pl.when(j < blocks[slot])
             def _():
-                def rows_of(r, c):
-                    tile(k, j, slot, pl.multiple_of(r * TILE, TILE), tok, False)
-                    return c
-
-                lax.fori_loop(0, tok // TILE, rows_of, 0)
+                attend(slot, False)
 
             @pl.when(j == blocks[slot])
             def _():
-                for r in range(tok // TILE):
-                    tile(k, j, slot, r * TILE, (r + 1) * TILE, True)
+                attend(slot, True)
 
         return carry
 
@@ -417,6 +462,9 @@
     kv = jnp.stack([
         jnp.concatenate([key_rows[:, :64], value_rows[:, :64]], axis=1),
         jnp.concatenate([key_rows[:, 64:], value_rows[:, 64:]], axis=1),
+    ])
+    packed = jnp.stack([
+        jnp.concatenate([queries[:tok // 2, s:s + 64], queries[tok // 2:, s:s + 64]], axis=1) for s in (0, 64)
     ])
     gate = cum_gate.reshape(2, 16, 1, tok)
     sp, tp = lax.axis_index("sp"), lax.axis_index("tp")
@@ -445,9 +493,12 @@
         in_specs=[vmem] * 7 + [smem] * 3 + [anywhere] * 4,
         out_specs=vmem,
         scratch_shapes=[
-            pltpu.VMEM((2, tok, 128), bf16),
-            pltpu.VMEM((2, tok, 128), bf16),
-            pltpu.VMEM((16, tok, 128), bf16),
+            pltpu.VMEM((2, tok // 2, 128), jnp.bfloat16),
+            pltpu.VMEM((2, tok, 256), jnp.bfloat16),
+            pltpu.VMEM((16, tok, 128), jnp.bfloat16),
+            pltpu.VMEM((16, tok, 128), jnp.bfloat16),
+            pltpu.VMEM((tok, 256), jnp.bfloat16),
+            pltpu.VMEM((4, TILE, tok), jnp.float32),
             pltpu.VMEM((tok, 128), bf16),
             pltpu.VMEM((2, 16, 1, tok), f32),
             pltpu.VMEM((2, tok, 128), f32),
@@ -476,7 +527,7 @@
         compiler_params=pltpu.CompilerParams(has_side_effects=True, vmem_limit_bytes=60 * 1024 * 1024),
         name="layer",
     )(
-        queries, kv, gate, residual, gain_mix.reshape(1, -1), gain_pre.reshape(1, -1),
+        packed, kv, gate, residual, gain_mix.reshape(1, -1), gain_pre.reshape(1, -1),
         gain_post.reshape(1, -1), token, place.reshape(128, 2), route_weight,
         out_weight, w_gate[0], w_up[0], w_down[0],
     )

time: 161 us -> 126 us (0.78)
  Pallas kernels: 151 us -> 116 us
    pallas_call x1, Pallas kernels: 151 us -> 116 us  [local(): pl.pallas_call(layer_kernel, out_shape=jax.ShapeDtypeStruct((128, 2048),...]
where the time goes in v3:
time: 126 us
  Pallas kernels  116 us (92%)
  local copies, waits for them, and re-layouts  5.58 us (4%)
  other arithmetic  3.95 us (3%)
    pallas_call x1, Pallas kernels, local(): pl.pallas_call(layer_kernel, out_shape=jax.ShapeDtypeStruct((128, 2048),...  116 us
    unnamed x13, local copies, waits for them, and re-layouts  2.76 us

profile of v3, /device:TPU:1, one launch (start us, length us, event | category | flops | bytes accessed | tf_op | source)
XLA Modules:
  0.0 125.9 jit_solution(6417556102057342626)
XLA Ops:
  0.0 0.0 copy-start
  0.0 0.0 copy-start.1
  0.0 1.3 %fusion.45 = (bf16[512,64]{1,0:T(8,128)(2,1)S(1)}, bf16[512,64]{1,0:T(8,128)(2,1)S(1)}, bf16[512,64]{1,0:T(8,128)(2,1)S(1)}, bf16[512,64]{1,0:T(8,128)(2,1)S(1)}) fusion(bf16[1024,128]{1,0:T(8,128)(2,1)} %param.14), kind=kLoop, calls=%fused_computation.130 | loop fusion | bytes 524288 | tf_op jit(solution)/shard_map/slice | solution.py:467
  1.3 0.1 maximum_bitcast_fusion.2
  1.5 0.7 pad_maximum_fusion.1.q_ref
  2.2 0.0 copy-done
  2.2 0.1 fusion.44
  2.3 0.0 copy-start.2
  2.3 0.0 copy-start.3
  2.3 0.0 copy-done.1
  2.3 0.0 copy-start.4
  2.4 0.1 fusion.43
  2.5 0.3 maximum_bitcast_fusion
  2.8 0.8 pad_maximum_fusion.kv_ref
  3.6 0.0 copy-done.2
  3.6 0.9 reshape.244.gate_ref
  4.5 0.0 copy-done.3
  4.5 0.1 copy.32
  4.6 0.1 reshape.248
  4.8 0.2 convert_reduce_fusion
  5.0 0.1 and_select_fusion
  5.0 0.7 select_reduce_fusion.token_ref
  5.8 0.1 reduce_sum.22
  5.9 0.1 copy.38
  6.1 1.0 fusion.21.place_ref
  7.0 0.0 copy-done.4
  7.0 0.7 copy.40.weight_ref
  7.8 116.2 %layer.1 = bf16[128,2048]{1,0:T(8,128)(2,1)} custom-call(bf16[2,512,128]{2,1,0:T(8,128)(2,1)} %pad_maximum_fusion.1.q_ref, bf16[2,1024,128]{2,1,0:T(8,128)(2,1)} %pad_maximum_fusion.kv_ref, f32[2,16,1,1024]{3,2,1,0:T(1,128)} %reshape.244.gate_ref, bf16[128,2048]{1,0:T(8,128)(2,1)} %residual_ref.1, f32[1,2048]{1,0:T(1,128)} %bitcast.17, f32[1,2048]{1,0:T(1,128)} %bitcast.18, ...), custom_call_target="tpu_custom_call" | custom-call | tf_op jit(solution)/shard_map/layer/pallas_call | solution.py:490
  124.0 1.9 %copy.50 = bf16[128,2048]{1,0:T(8,128)(2,1)} copy(bf16[128,2048]{1,0:T(8,128)(2,1)} %layer.1) | data formatting | bytes 1048576
  (1 shorter events, 0.0 us)
Async XLA Ops:
  0.0 2.2 %copy-start = (bf16[1024,128]{1,0:T(8,128)(2,1)S(1)}, bf16[1024,128]{1,0:T(8,128)(2,1)}, u32[]{:S(2)}) copy-start(bf16[1024,128]{1,0:T(8,128)(2,1)} %param.16) | copy-start | bytes 786436
  0.0 2.3 %copy-start.1 = (bf16[1024,128]{1,0:T(8,128)(2,1)S(1)}, bf16[1024,128]{1,0:T(8,128)(2,1)}, u32[]{:S(2)}) copy-start(bf16[1024,128]{1,0:T(8,128)(2,1)} %param.15) | copy-start | bytes 786436
  2.3 1.3 %copy-start.2 = (f32[2,16384]{1,0:T(2,128)S(1)}, f32[2,16384]{1,0:T(2,128)}, u32[]{:S(2)}) copy-start(f32[2,16384]{1,0:T(2,128)} %param.17) | copy-start | bytes 393220
  2.3 2.2 %copy-start.3 = (s32[128,2]{0,1:T(2,128)S(1)}, s32[128,2]{0,1:T(2,128)}, u32[]{:S(2)}) copy-start(s32[128,2]{0,1:T(2,128)} %param.23) | copy-start | bytes 3076
  2.3 4.7 %copy-start.4 = (f32[128,2]{0,1:T(2,128)S(1)}, f32[128,2]{0,1:T(2,128)}, u32[]{:S(2)}) copy-start(f32[128,2]{0,1:T(2,128)} %param.24) | copy-start | bytes 3076

commit v4 on v3

--- a/solution.py
+++ b/solution.py
@@ -42,22 +42,15 @@
     return low, (mid + low) % 4, (high + mid + low) % 4, place // 64
 
 
-def place_of(dz, dx, dy, dcore):
-    mid = (dx - dz + 4) % 4
-    high = (dy - dz - mid + 8) % 4
-    return dz + 4 * mid + 16 * high + 64 * dcore
-
-
 def layer_kernel(
-    q_ref, kv_ref, gate_ref, residual_ref, mix_ref, pre_ref, post_ref,
-    token_ref, place_ref, weight_ref, ow_hbm, wg_hbm, wu_hbm, wd_hbm, out_ref,
-    q_in, q_use, kv_buf, gate_cols, k_aug, s_buf, v_one, gate_buf, peak, acc, o_out, o_in, att,
+    q_raw, k_raw, v_raw, gate_ref, ids_ref, residual_ref, mix_ref, pre_ref, post_ref, weight_ref, ow_hbm, wg_hbm, wu_hbm, wd_hbm, out_ref,
+    q_ref, kv_ref, tables, scalars, q_in, q_use, kv_buf, gate_cols, k_aug, s_buf, v_one, gate_buf, peak, acc, o_out, o_in, att,
     ow, wg, wu, wd, slab_wide, slab, stream, outgoing, arrived_rows, results, returned,
     x_wide, x_rows, y_wide,
     kv_send, kv_recv, fwd_send, fwd_recv, q_send, q_recv, gate_send, gate_recv, o_send, o_recv,
-    w_sem, go_send, go_recv, back_send, back_recv,
+    table_sem, w_sem, go_send, go_recv, back_send, back_recv,
 ):
-    tok = kv_ref.shape[1]
+    tok = k_raw.shape[0]
     half = tok // 2
     sp, tp = lax.axis_index("sp"), lax.axis_index("tp")
     z, x = sp // 4, sp % 4
@@ -84,6 +77,35 @@
     for load in loads:
         load.start()
 
+    def peer(place, sign):
+        dz, dx, dy, dcore = offset_of(place)
+        return (
+            4 * ((z + sign * dz + 4) % 4) + (x + sign * dx + 4) % 4,
+            2 * ((y + sign * dy + 4) % 4) + (core + dcore) % 2,
+        )
+
+    barrier = pltpu.get_barrier_semaphore()
+
+    for d_tp in range(8):
+        other_tp = (tp + d_tp) % 8
+        for d_sp in range(16):
+            if d_sp + d_tp > 0:
+                pl.semaphore_signal(barrier, inc=1, **where((sp + d_sp) % 16, other_tp))
+
+    for r in range(0, tok, QROWS):
+        rows = slice(r, r + QROWS)
+        left = lax.broadcasted_iota(jnp.int32, (QROWS, 128), 1) < HEAD_DIM
+        keys, values = k_raw[rows, :].astype(jnp.float32), v_raw[rows, :].astype(jnp.float32)
+        kv_ref[0, rows, :] = jnp.where(left, keys, pltpu.roll(values, 64, 1)).astype(jnp.bfloat16)
+        kv_ref[1, rows, :] = jnp.where(left, pltpu.roll(keys, 64, 1), values).astype(jnp.bfloat16)
+        if r < half:
+            top = q_raw[rows, :].astype(jnp.float32)
+            low = q_raw[half + r:half + r + QROWS, :].astype(jnp.float32)
+            q_ref[0, rows, :] = jnp.where(left, top, pltpu.roll(low, 64, 1)).astype(jnp.bfloat16)
+            q_ref[1, rows, :] = jnp.where(left, pltpu.roll(top, 64, 1), low).astype(jnp.bfloat16)
+
+    pl.semaphore_wait(barrier, 127)
+
     q_copies = []
     for side in range(2):
         dest_sp = 4 * jnp.where(core == 0, zl, zh) + (xl if side == 0 else xh)
@@ -140,6 +162,36 @@
 
     lax.fori_loop(1, 9, send_kv, 0)
 
+    at_sub = lax.broadcasted_iota(jnp.int32, (128, 128), 0)
+    at_lane = lax.broadcasted_iota(jnp.int32, (128, 128), 1)
+    rows_of = [ids_ref[e:e + 1, :] for e in range(2)]
+    columns_of = [jnp.sum(jnp.where(at_sub == at_lane, r, 0), axis=1, keepdims=True) for r in rows_of]
+    spots = []
+    for ids in rows_of:
+        earlier = jnp.zeros((128, 128), jnp.int32)
+        for c in columns_of:
+            earlier = earlier + jnp.where((c == ids) & (at_sub < at_lane), 1, 0)
+        rank = jnp.sum(earlier, axis=0, keepdims=True)
+        dz = ((ids >> 5) - z + 4) & 3
+        dx = ((ids >> 3) - x + 4) & 3
+        dy = ((ids >> 1) - y + 4) & 3
+        dcore = (ids + core) & 1
+        mid = (dx - dz + 4) & 3
+        high = (dy - dz - mid + 8) & 3
+        spot = (dz + 4 * mid + 16 * high + 64 * dcore) * SLOTS + rank
+        spots.append(jnp.minimum(spot, 128 * SLOTS - 1))
+    slot_row = lax.broadcasted_iota(jnp.int32, (128, 128 * SLOTS), 1)
+    slot_sub = lax.broadcasted_iota(jnp.int32, (128, 128 * SLOTS), 0)
+    token = jnp.zeros((128, 128 * SLOTS), jnp.int32)
+    for spot in spots:
+        column = jnp.sum(jnp.where(at_sub == at_lane, spot, 0), axis=1, keepdims=True)
+        token = token + jnp.where(column == slot_row, slot_sub, 0)
+    tables[0:1, :] = jnp.minimum(jnp.sum(token, axis=0, keepdims=True), 127)
+    tables[1:2, 0:128] = spots[0]
+    tables[2:3, 0:128] = spots[1]
+    table_copy = pltpu.make_async_copy(tables, scalars, table_sem)
+    table_copy.start()
+
     def arrived(k):
         rows = pl.ds(core * half, half)
         return copy(kv_buf.at[k, rows], kv_buf.at[k, rows], kv_send.at[0, 0], kv_recv.at[k], sp, partner)
@@ -167,8 +219,12 @@
     ).astype(jnp.bfloat16)
     row8 = lax.broadcasted_iota(jnp.int32, (8, tok), 0)
 
+    def gate_row(j):
+        span = pl.ds(pl.multiple_of(j * tok, tok), tok)
+        return jnp.where(bx == 0, gate_buf[0:1, span], gate_buf[1:2, span])
+
     def columns(j, carry):
-        parts = split3(gate_buf[bx, j] * -LOG2E)
+        parts = split3(gate_row(j) * -LOG2E)
         stack = jnp.where(row8 == 3, 1.0, 0.0)
         for i in range(3):
             stack = jnp.where(row8 == i, parts[i], stack)
@@ -187,7 +243,7 @@
         def _():
             copy(q_ref.at[0], q_in.at[slot], q_send.at[0], q_recv.at[slot], sp, partner).wait_recv()
 
-        base = gate_buf[bx, blocks[slot], :, 0:1] * LOG2E
+        base = gate_row(blocks[slot])[:, 0:1] * LOG2E
         pieces = split3(base)
         for r in range(tok // QROWS):
             rows = pl.ds(r * QROWS, QROWS)
@@ -278,22 +334,28 @@
     def o_copy(slot, t):
         return copy(o_out.at[slot, t], o_in.at[head], o_send.at[slot, t], o_recv.at[head], blocks[slot], t)
 
-    for slot in range(2):
-        for t in range(8):
-            o = acc[slot, t * 128:(t + 1) * 128, :]
-            o = o / pltpu.roll(o, 64, 1)
-            o_out[slot, t] = jnp.where(lane64 < 64, pltpu.roll(o[0:64], 64, 1), o[64:128]).astype(jnp.bfloat16)
-    for slot in range(2):
-        for t in range(8):
-            mine = (blocks[slot] == sp) & (tp == t)
-
-            @pl.when(mine)
-            def _():
-                o_in[head] = o_out[slot, t]
-
-            @pl.when(jnp.logical_not(mine))
-            def _():
-                o_copy(slot, t).start()
+    pieces_out = [(slot, t) for slot in range(2) for t in range(8)]
+
+    def start_o(slot, t):
+        mine = (blocks[slot] == sp) & (tp == t)
+
+        @pl.when(mine)
+        def _():
+            o_in[head] = o_out[slot, t]
+
+        @pl.when(jnp.logical_not(mine))
+        def _():
+            o_copy(slot, t).start()
+
+    for i, (slot, t) in enumerate(pieces_out):
+        o = acc[slot, t * 128:(t + 1) * 128, :]
+        o = o / pltpu.roll(o, 64, 1)
+        o_out[slot, t] = jnp.where(lane64 < 64, pltpu.roll(o[0:64], 64, 1), o[64:128]).astype(jnp.bfloat16)
+        if i % 4 == 3 and i > 3:
+            for piece in pieces_out[i - 7:i - 3]:
+                start_o(*piece)
+    for piece in pieces_out[12:]:
+        start_o(*piece)
 
     for h in range(16):
         r = h % 4
@@ -322,20 +384,6 @@
         slab_wide[pl.ds(c, 128, stride=16), :] = normed[:, c * 128:(c + 1) * 128]
     slab[...] = slab_wide[...].reshape(128, 16, 128).astype(jnp.bfloat16)
 
-    def fill(place, carry):
-        for s in range(SLOTS):
-            outgoing[place * SLOTS + s] = slab[token_ref[place * SLOTS + s]]
-        return carry
-
-    lax.fori_loop(0, 128, fill, 0, unroll=4)
-
-    def peer(place, sign):
-        dz, dx, dy, dcore = offset_of(place)
-        return (
-            4 * ((z + sign * dz + 4) % 4) + (x + sign * dx + 4) % 4,
-            2 * ((y + sign * dy + 4) % 4) + (core + dcore) % 2,
-        )
-
     def go(place):
         rows = pl.ds(place * SLOTS, SLOTS)
         return copy(
@@ -348,11 +396,21 @@
             results.at[rows], returned.at[rows], back_send, back_recv.at[place // GROUP], *peer(place, -1)
         )
 
+    def fill(place, carry):
+        for s in range(SLOTS):
+            outgoing[place * SLOTS + s] = slab[scalars[0, place * SLOTS + s]]
+        return carry
+
     def start_go(place, carry):
         go(place).start()
         return carry
 
-    lax.fori_loop(1, 128, start_go, 0)
+    table_copy.wait()
+    for first in range(0, 128 + 16, 16):
+        if first < 128:
+            lax.fori_loop(first, first + 16, fill, 0, unroll=4)
+        if first > 0:
+            lax.fori_loop(max(1, first - 16), first, start_go, 0)
     arrived_rows[0:SLOTS] = outgoing[0:SLOTS]
     for load in loads[1:]:
         load.wait()
@@ -396,8 +454,8 @@
         ).wait_recv()
 
     def combine(n, carry):
-        first = returned[place_ref[n, 0]].astype(jnp.float32) * weight_ref[n, 0]
-        second = returned[place_ref[n, 1]].astype(jnp.float32) * weight_ref[n, 1]
+        first = returned[scalars[1, n]].astype(jnp.float32) * weight_ref[0, n]
+        second = returned[scalars[2, n]].astype(jnp.float32) * weight_ref[1, n]
         slab_wide[pl.ds(pl.multiple_of(n * 16, 16), 16), :] = first + second
         return carry
 
@@ -459,28 +517,6 @@
     w_down,
 ):
     tok = queries.shape[0]
-    kv = jnp.stack([
-        jnp.concatenate([key_rows[:, :64], value_rows[:, :64]], axis=1),
-        jnp.concatenate([key_rows[:, 64:], value_rows[:, 64:]], axis=1),
-    ])
-    packed = jnp.stack([
-        jnp.concatenate([queries[:tok // 2, s:s + 64], queries[tok // 2:, s:s + 64]], axis=1) for s in (0, 64)
-    ])
-    gate = cum_gate.reshape(2, 16, 1, tok)
-    sp, tp = lax.axis_index("sp"), lax.axis_index("tp")
-    flat = route_ids.reshape(-1)
-    order = lax.iota(jnp.int32, flat.shape[0])
-    earlier = (flat[None, :] == flat[:, None]) & (order[None, :] < order[:, None])
-    rank = jnp.sum(earlier.astype(jnp.int32), axis=1)
-    e_sp, e_tp = flat // 8, flat % 8
-    place = place_of(
-        (e_sp // 4 - sp // 4 + 4) % 4,
-        (e_sp % 4 - sp % 4 + 4) % 4,
-        (e_tp // 2 - tp // 2 + 4) % 4,
-        (e_tp % 2 + tp % 2) % 2,
-    ) * SLOTS + rank
-    slots = lax.iota(jnp.int32, 128 * SLOTS)
-    token = jnp.sum(jnp.where(slots[:, None] == place[None, :], order[None, :] // 2, 0), axis=1)
     dma = pltpu.SemaphoreType.DMA
     vmem, smem, anywhere = (
         pl.BlockSpec(memory_space=space) for space in (pltpu.VMEM, pltpu.SMEM, pl.ANY)
@@ -490,17 +526,21 @@
     return pl.pallas_call(
         layer_kernel,
         out_shape=jax.ShapeDtypeStruct((128, 2048), bf16),
-        in_specs=[vmem] * 7 + [smem] * 3 + [anywhere] * 4,
+        in_specs=[vmem] * 9 + [smem] + [anywhere] * 4,
         out_specs=vmem,
         scratch_shapes=[
-            pltpu.VMEM((2, tok // 2, 128), jnp.bfloat16),
-            pltpu.VMEM((2, tok, 256), jnp.bfloat16),
+            pltpu.VMEM((2, tok // 2, 128), bf16),
+            pltpu.VMEM((2, tok, 128), bf16),
+            pltpu.VMEM((8, 128 * SLOTS), jnp.int32),
+            pltpu.SMEM((8, 128 * SLOTS), jnp.int32),
+            pltpu.VMEM((2, tok // 2, 128), bf16),
+            pltpu.VMEM((2, tok, 256), bf16),
             pltpu.VMEM((16, tok, 128), jnp.bfloat16),
             pltpu.VMEM((16, tok, 128), jnp.bfloat16),
             pltpu.VMEM((tok, 256), jnp.bfloat16),
             pltpu.VMEM((4, TILE, tok), jnp.float32),
             pltpu.VMEM((tok, 128), bf16),
-            pltpu.VMEM((2, 16, 1, tok), f32),
+            pltpu.VMEM((2, 16 * tok), f32),
             pltpu.VMEM((2, tok, 128), f32),
             pltpu.VMEM((2, tok, 128), f32),
             pltpu.VMEM((2, 8, 64, 128), bf16),
@@ -522,13 +562,13 @@
             pltpu.VMEM((rows * 16, 128), f32),
             dma((16, 2)), dma((16,)), dma((16,)), dma((16,)), dma((2,)), dma((2,)), dma, dma,
             dma((2, 8)), dma((16,)),
-            dma((4,)), dma, dma((128 // GROUP,)), dma, dma((128 // GROUP,)),
+            dma, dma((4,)), dma, dma((128 // GROUP,)), dma, dma((128 // GROUP,)),
         ],
-        compiler_params=pltpu.CompilerParams(has_side_effects=True, vmem_limit_bytes=60 * 1024 * 1024),
+        compiler_params=pltpu.CompilerParams(collective_id=0, has_side_effects=True, vmem_limit_bytes=60 * 1024 * 1024),
         name="layer",
     )(
-        packed, kv, gate, residual, gain_mix.reshape(1, -1), gain_pre.reshape(1, -1),
-        gain_post.reshape(1, -1), token, place.reshape(128, 2), route_weight,
+        queries, key_rows, value_rows, cum_gate, route_ids.T, residual, gain_mix.reshape(1, -1),
+        gain_pre.reshape(1, -1), gain_post.reshape(1, -1), route_weight.T,
         out_weight, w_gate[0], w_up[0], w_down[0],
     )
 

time: 126 us -> 116 us (0.921)
  the two profiles are of different devices: /device:TPU:1 before, /device:TPU:27 now
where the time goes in v4:
time: 116 us
  Pallas kernels  114 us (98%)
  local copies, waits for them, and re-layouts  1.88 us (2%)
    pallas_call x1, Pallas kernels, local(): pl.pallas_call(layer_kernel, out_shape=jax.ShapeDtypeStruct((128, 2048),...  114 us

profile of v4, /device:TPU:27, one launch (start us, length us, event | category | flops | bytes accessed | tf_op | source)
XLA Modules:
  0.0 115.7 jit_solution(12677043484822087511)
XLA Ops:
  0.0 113.8 %layer.1 = bf16[128,2048]{1,0:T(8,128)(2,1)} custom-call(bf16[1024,128]{1,0:T(8,128)(2,1)} %q_raw.1, bf16[1024,128]{1,0:T(8,128)(2,1)} %k_raw.1, bf16[1024,128]{1,0:T(8,128)(2,1)} %v_raw.1, f32[2,16384]{1,0:T(2,128)} %gate_ref.1, s32[2,128]{1,0:T(2,128)} %bitcast.14, bf16[128,2048]{1,0:T(8,128)(2,1)} %residual_ref.1, f32[1,2048]{1,0:T(1,128)} %bitcast.11, ...), custom_call_target="tpu_custom_call" | custom-call | tf_op jit(solution)/shard_map/layer/pallas_call | solution.py:526
  113.8 1.9 %copy.16 = bf16[128,2048]{1,0:T(8,128)(2,1)} copy(bf16[128,2048]{1,0:T(8,128)(2,1)} %layer.1) | data formatting | bytes 1048576

commit v5 on v4

--- a/solution.py
+++ b/solution.py
@@ -18,7 +18,7 @@
 TILE = 256
 QROWS = 256
 SLOTS = 3
-GROUP = 32
+GROUP = 64
 
 
 def rms_scale(rows, gain):
@@ -233,7 +233,7 @@
         ).astype(jnp.bfloat16)
         return carry
 
-    lax.fori_loop(0, 16, columns, 0)
+    lax.fori_loop(0, 16, columns, 0, unroll=4)
     for slot in range(2):
         from_x = jnp.where(core == slot, xl, xh)
         from_sp = 4 * (zl if slot == 0 else zh) + from_x

time: 116 us -> 113 us (0.974)
  the two profiles are of different devices: /device:TPU:27 before, /device:TPU:1 now
where the time goes in v5:
time: 113 us
  Pallas kernels  111 us (98%)
  local copies, waits for them, and re-layouts  1.88 us (2%)
    pallas_call x1, Pallas kernels, local(): pl.pallas_call(layer_kernel, out_shape=jax.ShapeDtypeStruct((128, 2048),...  111 us

profile of v5, /device:TPU:1, one launch (start us, length us, event | category | flops | bytes accessed | tf_op | source)
XLA Modules:
  0.0 112.8 jit_solution(11871651487715675179)
XLA Ops:
  0.0 110.9 %layer.1 = bf16[128,2048]{1,0:T(8,128)(2,1)} custom-call(bf16[1024,128]{1,0:T(8,128)(2,1)} %q_raw.1, bf16[1024,128]{1,0:T(8,128)(2,1)} %k_raw.1, bf16[1024,128]{1,0:T(8,128)(2,1)} %v_raw.1, f32[2,16384]{1,0:T(2,128)} %gate_ref.1, s32[2,128]{1,0:T(2,128)} %bitcast.14, bf16[128,2048]{1,0:T(8,128)(2,1)} %residual_ref.1, f32[1,2048]{1,0:T(1,128)} %bitcast.11, ...), custom_call_target="tpu_custom_call" | custom-call | tf_op jit(solution)/shard_map/layer/pallas_call | solution.py:526
  110.9 1.9 %copy.16 = bf16[128,2048]{1,0:T(8,128)(2,1)} copy(bf16[128,2048]{1,0:T(8,128)(2,1)} %layer.1) | data formatting | bytes 1048576

commit v6 on v5

--- a/solution.py
+++ b/solution.py
@@ -408,7 +408,7 @@
     table_copy.wait()
     for first in range(0, 128 + 16, 16):
         if first < 128:
-            lax.fori_loop(first, first + 16, fill, 0, unroll=4)
+            lax.fori_loop(first, first + 16, fill, 0, unroll=16)
         if first > 0:
             lax.fori_loop(max(1, first - 16), first, start_go, 0)
     arrived_rows[0:SLOTS] = outgoing[0:SLOTS]
@@ -459,7 +459,7 @@
         slab_wide[pl.ds(pl.multiple_of(n * 16, 16), 16), :] = first + second
         return carry
 
-    lax.fori_loop(0, 128, combine, 0, unroll=4)
+    lax.fori_loop(0, 128, combine, 0, unroll=16)
     combined = jnp.concatenate(
         [slab_wide[pl.ds(c, 128, stride=16), :] for c in range(16)], axis=1
     )

time: 113 us -> 113 us (level)
  no operation moved by 1% of the time
where the time goes in v6:
time: 113 us
  Pallas kernels  111 us (98%)
  local copies, waits for them, and re-layouts  1.88 us (2%)
    pallas_call x1, Pallas kernels, local(): pl.pallas_call(layer_kernel, out_shape=jax.ShapeDtypeStruct((128, 2048),...  111 us

profile of v6, /device:TPU:1, one launch (start us, length us, event | category | flops | bytes accessed | tf_op | source)
XLA Modules:
  0.0 112.5 jit_solution(7235941044228927072)
XLA Ops:
  0.0 110.7 %layer.1 = bf16[128,2048]{1,0:T(8,128)(2,1)} custom-call(bf16[1024,128]{1,0:T(8,128)(2,1)} %q_raw.1, bf16[1024,128]{1,0:T(8,128)(2,1)} %k_raw.1, bf16[1024,128]{1,0:T(8,128)(2,1)} %v_raw.1, f32[2,16384]{1,0:T(2,128)} %gate_ref.1, s32[2,128]{1,0:T(2,128)} %bitcast.14, bf16[128,2048]{1,0:T(8,128)(2,1)} %residual_ref.1, f32[1,2048]{1,0:T(1,128)} %bitcast.11, ...), custom_call_target="tpu_custom_call" | custom-call | tf_op jit(solution)/shard_map/layer/pallas_call | solution.py:526
  110.7 1.9 %copy.16 = bf16[128,2048]{1,0:T(8,128)(2,1)} copy(bf16[128,2048]{1,0:T(8,128)(2,1)} %layer.1) | data formatting | bytes 1048576
